TPU v7x, 32 devices: a whole 2x2x4 slice. The times are simulated.
32 devices in a mesh: ep: 8 (over z, x), tp: 4 (over y, core).
Axes of the slice: x: 2, y: 2, z: 4, core: 2. Of those that a mesh axis runs over, the one named last changes fastest.
Arguments:
- query_rows: bfloat16 [3072, 4096], P('ep', 'tp'), may hold values from -6 to 6
- key_rows: bfloat16 [3072, 2048], P('ep', 'tp'), may hold values from -6 to 6
- value_rows: bfloat16 [3072, 2048], P('ep', 'tp'), may hold values from -6 to 6
- query_gain: float32 [128], replicated, may hold values from 0.4 to 5
- key_gain: float32 [128], replicated, may hold values from 0.4 to 5
- w_out: bfloat16 [4096, 2048], P('tp'), may hold values from -0.09375 to 0.09375
- mixer_gain: float32 [2048], replicated, may hold values from 0.1 to 1.9
- expert_input: bfloat16 [1536, 2048], P('ep'), may hold values from -6 to 6
- expert_ids: int32 [1536, 2], P('ep'), may hold values from 0 to 7, as said below
- expert_weights: float32 [1536, 2], P('ep'), may hold values from 0.1 to 1
- input_gain: float32 [2048], replicated, may hold values from 0.1 to 1.9
- w_gate: bfloat16 [8, 2048, 4096], P('ep', None, 'tp'), may hold values from -0.125 to 0.125
- w_up: bfloat16 [8, 2048, 4096], P('ep', None, 'tp'), may hold values from -0.125 to 0.125
- w_down: bfloat16 [8, 4096, 2048], P('ep', 'tp'), may hold values from -2 to 2
- out_gain: float32 [2048], P('tp'), may hold values from 0.1 to 1.9
Outputs:
- mixer_result: bfloat16 [3072, 2048], P(('ep', 'tp'))
- moe_result: bfloat16 [1536, 2048], P('ep', 'tp')
Inputs may be any that keep to these rules, and one draw needn't show every extreme that they name: `expert_ids`: the two experts of a row differ and lie in one group of 2 consecutive experts. Among the rows of one index of ep (aligned blocks of 192 rows) no expert is named by more than 72 rows, and in every block some expert is named by exactly 72 rows.
All inputs are finite; a program needn't handle non-finite values.
Results may differ from a plain program's by a relative error of at most 0.02.
The roundings to bfloat16 on the way count: a program that leaves them out, or rounds other values in their place, can miss the bound.
Values may be sent and summed in bfloat16 or wider, within the bound.
A program may use at most 64 MiB of HBM per device.

v0:
```python
import functools
import math

import jax
import jax.numpy as jnp
from jax import lax
from jax.experimental import pallas as pl
from jax.experimental.pallas import tpu as pltpu
from jax.sharding import PartitionSpec as P

D = 2048
GRID = 64
GROUPS = 4
BLOCK_Q = 384
BLOCK_K = 768


EPS = 1e-06
THETA = 10000.0


def turn_half(half_part, position):
    half_width = half_part.shape[-1]
    frequency = THETA ** (-jnp.arange(0, half_width, 2, dtype=jnp.float32) / half_width)
    angles = position[:, None, None] * frequency[None, None, :]
    cosine = jnp.cos(angles)
    sine_part = jnp.sin(angles)
    first_half = half_part[..., : half_width // 2]
    second = half_part[..., half_width // 2 :]
    return jnp.concatenate(
        [first_half * cosine - second * sine_part, second * cosine + first_half * sine_part],
        axis=-1,
    )


def norm_turn(raw_rows, gain_vec, row_offset):
    row_count = raw_rows.shape[0]
    head_dim = gain_vec.shape[0]
    head_count = raw_rows.shape[1] // head_dim
    by_head = raw_rows.astype(jnp.float32).reshape(row_count, head_count, head_dim)
    scaled = (
        by_head * lax.rsqrt(jnp.mean(by_head * by_head, axis=-1, keepdims=True) + EPS) * gain_vec
    )
    position = row_offset + jnp.arange(row_count, dtype=jnp.int32)
    grid_row = (position // GRID).astype(jnp.float32)
    grid_col = (position % GRID).astype(jnp.float32)
    half_dim = head_dim // 2
    turned = jnp.concatenate(
        [turn_half(scaled[..., :half_dim], grid_row), turn_half(scaled[..., half_dim:], grid_col)],
        axis=-1,
    )
    return turned.reshape(row_count, head_count * head_dim).astype(jnp.bfloat16)


def attend_block(scale, block_keys, query, k_ref, k_cols, vt_ref):
    columns, head_dim = query.shape
    steps = k_ref.shape[0] // block_keys

    def step(index, carry):
        top, total, acc = carry
        rows = pl.ds(pl.multiple_of(index * block_keys, block_keys), block_keys)
        scores = (
            lax.dot_general(
                k_ref[rows, k_cols],
                query,
                (((1,), (1,)), ((), ())),
                preferred_element_type=jnp.float32,
            )
            * scale
        )
        new_top = jnp.maximum(top, jnp.max(scores, axis=0, keepdims=True))
        exponent = jnp.exp2(scores - new_top)
        factor = jnp.exp2(top - new_top)
        total = total * factor + jnp.sum(exponent, axis=0, keepdims=True)
        acc = acc * factor + jnp.dot(
            vt_ref[:, rows], exponent.astype(jnp.bfloat16), preferred_element_type=jnp.float32
        )
        return new_top, total, acc

    carry = (
        jnp.full((1, columns), -1e30, jnp.float32),
        jnp.zeros((1, columns), jnp.float32),
        jnp.zeros((head_dim, columns), jnp.float32),
    )
    if steps <= 8:
        for index in range(steps):
            carry = step(index, carry)
    else:
        carry = lax.fori_loop(0, steps, step, carry)
    _, total, acc = carry
    return (acc / total).T.astype(jnp.bfloat16)


def attend_kernel(scale, block_keys, q_ref, k_ref, v_ref, o_ref, vt_ref):
    @pl.when(pl.program_id(1) == 0)
    def _():
        vt_ref[...] = v_ref[...].T

    o_ref[...] = attend_block(scale, block_keys, q_ref[...], k_ref, slice(None), vt_ref)


def attend_send_kernel(
    n_ep, scale, block_keys, packed, out, vt_ref, stage, send_sem, recv_sem, own_sem
):
    me = lax.axis_index("ep")
    row_count = out.shape[0]
    head_dim = vt_ref.shape[0]
    barrier = pltpu.get_barrier_semaphore()
    for offset in range(1, n_ep):
        pl.semaphore_signal(
            barrier,
            inc=1,
            device_id={"ep": lax.rem(me + offset, n_ep)},
            device_id_type=pl.DeviceIdType.MESH,
        )
    pl.semaphore_wait(barrier, n_ep - 1)
    columns = pl.ds(pl.multiple_of(me * head_dim, head_dim), head_dim)

    def send(offset):
        return pltpu.make_async_remote_copy(
            src_ref=stage.at[offset - 1],
            dst_ref=out.at[:, columns],
            send_sem=send_sem.at[offset - 1],
            recv_sem=recv_sem.at[offset - 1],
            device_id={"ep": lax.rem(me + offset, n_ep)},
            device_id_type=pl.DeviceIdType.MESH,
        )

    vt_ref[...] = packed[:, 2 * head_dim : 3 * head_dim].T

    def block(index, carry):
        @pl.when(index > 0)
        def _():
            send(index).start()

        owner = lax.rem(me + index + 1, n_ep)
        rows = pl.ds(pl.multiple_of(owner * row_count, row_count), row_count)
        stage[index] = attend_block(
            scale,
            block_keys,
            packed[rows, 0:head_dim],
            packed,
            slice(head_dim, 2 * head_dim),
            vt_ref,
        )
        return carry

    lax.fori_loop(0, n_ep, block, 0)
    own = pltpu.make_async_copy(stage.at[n_ep - 1], out.at[:, columns], own_sem)
    own.start()
    for offset in range(1, n_ep):
        send(offset).wait()
    own.wait()


def attend_send(packed, n_ep, head_dim):
    tokens = packed.shape[0]
    row_count = tokens // n_ep
    return pl.pallas_call(
        functools.partial(
            attend_send_kernel,
            n_ep,
            head_dim**-0.5 * math.log2(math.e),
            divisor(tokens, BLOCK_K),
        ),
        in_specs=[pl.BlockSpec(memory_space=pltpu.VMEM)],
        out_specs=pl.BlockSpec(memory_space=pltpu.VMEM),
        out_shape=jax.ShapeDtypeStruct((row_count, n_ep * head_dim), jnp.bfloat16),
        scratch_shapes=[
            pltpu.VMEM((head_dim, tokens), jnp.bfloat16),
            pltpu.VMEM((n_ep, row_count, head_dim), jnp.bfloat16),
            pltpu.SemaphoreType.DMA((n_ep - 1,)),
            pltpu.SemaphoreType.DMA((n_ep - 1,)),
            pltpu.SemaphoreType.DMA,
        ],
        compiler_params=pltpu.CompilerParams(collective_id=0, has_side_effects=True),
        cost_estimate=pl.CostEstimate(
            flops=8 * tokens * tokens * head_dim,
            bytes_accessed=8 * tokens * head_dim,
            transcendentals=tokens * tokens,
        ),
        name="attend_send",
    )(packed)


def divisor(size, limit):
    block = limit
    while size % block:
        block -= 128
    return block


def attend(query, key, value, heads, head_dim, group_size, q_col, k_col, v_col):
    tokens = query.shape[0]
    keys = key.shape[0]
    block_q = divisor(tokens, BLOCK_Q)
    block_k = divisor(keys, BLOCK_K)
    flops = 4 * heads * tokens * keys * head_dim
    return pl.pallas_call(
        functools.partial(attend_kernel, head_dim**-0.5 * math.log2(math.e), block_k),
        grid=(heads, tokens // block_q),
        in_specs=[
            pl.BlockSpec((block_q, head_dim), lambda h, i: (i, q_col + h)),
            pl.BlockSpec((keys, head_dim), lambda h, i: (0, k_col + h // group_size)),
            pl.BlockSpec((keys, head_dim), lambda h, i: (0, v_col + h // group_size)),
        ],
        out_specs=pl.BlockSpec((block_q, head_dim), lambda h, i: (i, h)),
        out_shape=jax.ShapeDtypeStruct((tokens, heads * head_dim), jnp.bfloat16),
        scratch_shapes=[pltpu.VMEM((head_dim, keys), jnp.bfloat16)],
        compiler_params=pltpu.CompilerParams(dimension_semantics=("arbitrary", "arbitrary")),
        cost_estimate=pl.CostEstimate(
            flops=2 * flops,
            bytes_accessed=8 * tokens * heads * head_dim,
            transcendentals=heads * tokens * keys,
        ),
        name="attend",
    )(query, key, value)


def mixer_half(query_rows, key_rows, value_rows, query_gain, key_gain, w_out, mixer_gain):
    row_count = query_rows.shape[0]
    head_dim = query_gain.shape[0]
    n_ep = lax.axis_size("ep")
    row_offset = lax.axis_index("ep") * row_count
    query_turned = norm_turn(query_rows, query_gain, row_offset)
    key_turned = norm_turn(key_rows, key_gain, row_offset)
    local_heads = query_rows.shape[1] // head_dim
    group_size = query_rows.shape[1] // key_rows.shape[1]
    if local_heads == n_ep:
        by_head = [
            x.reshape(row_count, -1, head_dim).transpose(1, 0, 2)
            for x in (query_turned, key_turned, value_rows)
        ]
        outgoing = jnp.concatenate(
            [by_head[0]] + [jnp.repeat(x, group_size, axis=0) for x in by_head[1:]], axis=2
        )
        arrived = lax.all_to_all(outgoing, "ep", split_axis=0, concat_axis=0, tiled=True)
        packed = arrived.reshape(n_ep * row_count, 3 * head_dim)
        attended = attend_send(packed, n_ep, head_dim)
    else:
        key_all = lax.all_gather(key_turned, "ep", axis=0, tiled=True)
        value_all = lax.all_gather(value_rows, "ep", axis=0, tiled=True)
        attended = attend(
            query_turned, key_all, value_all, local_heads, head_dim, group_size, 0, 0, 0
        )
    mixed_sum = lax.psum_scatter(
        jnp.dot(attended, w_out, preferred_element_type=jnp.float32).astype(jnp.bfloat16),
        "tp",
        scatter_dimension=0,
        tiled=True,
    ).astype(jnp.float32)
    scaled = (
        mixed_sum
        * lax.rsqrt(jnp.mean(mixed_sum * mixed_sum, axis=1, keepdims=True) + EPS)
        * mixer_gain
    )
    return scaled.astype(jnp.bfloat16)


def expert_half(
    expert_input, expert_ids, expert_weights, input_gain, w_gate, w_up, w_down, out_gain
):
    row_count, width = expert_input.shape
    top_count = expert_ids.shape[1]
    n_tp = lax.axis_size("tp")
    expert_total = w_gate.shape[0] * lax.axis_size("ep")
    inner_count = expert_total // GROUPS
    capacity = 3 * row_count // (4 * inner_count)
    slots = expert_total * capacity
    inputs_f = expert_input.astype(jnp.float32)
    normed = (
        inputs_f
        * lax.rsqrt(jnp.mean(inputs_f * inputs_f, axis=1, keepdims=True) + EPS)
        * input_gain
    ).astype(jnp.bfloat16)
    row_index = jnp.arange(row_count, dtype=jnp.int32)
    before = row_index[None, :] < row_index[:, None]
    slot_index = jnp.arange(slots, dtype=jnp.int32)
    slot_of = []
    for k in range(top_count):
        same = jnp.zeros((row_count, row_count), bool)
        for other in range(top_count):
            same = same | (expert_ids[:, k][:, None] == expert_ids[:, other][None, :])
        rank = jnp.sum((same & before).astype(jnp.int32), axis=1)
        slot_of.append(expert_ids[:, k] * capacity + rank)
    chosen = [slot_index[:, None] == slot[None, :] for slot in slot_of]
    picker = functools.reduce(jnp.logical_or, chosen).astype(jnp.bfloat16)
    share = width // n_tp
    own = lax.dynamic_slice_in_dim(normed, lax.axis_index("tp") * share, share, axis=1)
    outgoing = jnp.dot(picker, own, preferred_element_type=jnp.float32).astype(jnp.bfloat16)
    arrived = lax.all_to_all(
        outgoing.reshape(expert_total, capacity, share),
        "ep",
        split_axis=0,
        concat_axis=0,
        tiled=True,
    ).reshape(slots, share)
    shares = lax.all_gather(arrived, "tp", axis=0, tiled=False)
    arrived = jnp.concatenate([shares[j] for j in range(n_tp)], axis=1)
    gate_pre = jnp.dot(arrived, w_gate[0], preferred_element_type=jnp.float32)
    up_pre = jnp.dot(arrived, w_up[0], preferred_element_type=jnp.float32)
    hidden = (jax.nn.silu(gate_pre) * up_pre).astype(jnp.bfloat16)
    partial_term = jnp.dot(hidden, w_down[0], preferred_element_type=jnp.float32)
    summed = lax.psum_scatter(
        partial_term.astype(jnp.bfloat16), "tp", scatter_dimension=1, tiled=True
    )
    returned = lax.all_to_all(summed, "ep", split_axis=0, concat_axis=0, tiled=True)
    combined = jnp.zeros((row_count, returned.shape[1]), jnp.float32)
    for k in range(top_count):
        select = (slot_of[k][:, None] == slot_index[None, :]).astype(jnp.bfloat16)
        picked = jnp.dot(select, returned, preferred_element_type=jnp.float32)
        combined = combined + picked * expert_weights[:, k][:, None]
    squares = lax.psum(jnp.sum(combined * combined, axis=1), "tp")
    scaled = combined * lax.rsqrt(squares / D + EPS)[:, None] * out_gain
    return scaled.astype(jnp.bfloat16)


def per_device(
    query_rows,
    key_rows,
    value_rows,
    query_gain,
    key_gain,
    w_out,
    mixer_gain,
    expert_input,
    expert_ids,
    expert_weights,
    input_gain,
    w_gate,
    w_up,
    w_down,
    out_gain,
):
    mixer_result = mixer_half(
        query_rows, key_rows, value_rows, query_gain, key_gain, w_out, mixer_gain
    )
    moe_result = expert_half(
        expert_input, expert_ids, expert_weights, input_gain, w_gate, w_up, w_down, out_gain
    )
    return (mixer_result, moe_result)


def solution(mesh):
    return jax.shard_map(
        per_device,
        mesh=mesh,
        in_specs=(
            P("ep", "tp"),
            P("ep", "tp"),
            P("ep", "tp"),
            P(),
            P(),
            P("tp", None),
            P(),
            P("ep", None),
            P("ep", None),
            P("ep", None),
            P(),
            P("ep", None, "tp"),
            P("ep", None, "tp"),
            P("ep", "tp", None),
            P("tp"),
        ),
        out_specs=(P(("ep", "tp"), None), P("ep", "tp")),
        check_vma=False,
    )
```

profile of v0, /device:TPU:0, one launch (start us, length us, event | category | flops | bytes accessed | tf_op | source)
XLA Modules:
  0.0 182.2 jit_solution(3168510102806947425)
XLA Ops:
  7.2 1.4 convert_element_type.65
  9.1 0.8 dynamic-slice
  9.9 0.4 convolution_convert_fusion.1
  10.3 23.8 %all_to_all.22 = bf16[8,72,512]{2,1,0:T(8,128)(2,1)} all-to-all(bf16[8,72,512]{2,1,0:T(8,128)(2,1)S(1)} %bitcast.59), channel_id=1, replica_groups=mesh['ep'=8,'tp'=4] {'ep'}, dimensions={0} | all-to-all | bytes 1179648 | tf_op jit(solution)/shard_map/all_to_all | solution.py:291
  34.2 0.4 copy.56
  34.6 0.4 multiply_cosine_fusion.1
  35.9 0.5 multiply_reduce_fusion.1
  36.4 0.5 multiply_multiply_fusion
  36.9 1.4 subtract_convert_fusion.1
  38.4 1.2 maximum_bitcast_fusion.1
  39.6 0.3 copy.65
  40.0 0.3 copy.66
  41.2 0.3 pad_maximum_fusion
  41.5 2.7 %copy.67 = bf16[8,384,384]{2,1,0:T(8,128)(2,1)} copy(bf16[8,384,384]{1,2,0:T(8,128)(2,1)S(1)} %pad_maximum_fusion) | data formatting | bytes 4718592 | tf_op jit(solution)/shard_map/concatenate | solution.py:234
  44.1 3.6 %all-to-all-start = ((bf16[8,384,384]{2,1,0:T(8,128)(2,1)}), bf16[8,384,384]{2,1,0:T(8,128)(2,1)S(1)}, u32[]{:S(2)}, u32[]{:S(2)}) async-start(bf16[8,384,384]{2,1,0:T(8,128)(2,1)} %copy.67), calls=%async_computation | async-start | bytes 4718592 | tf_op jit(solution)/shard_map/all_to_all | solution.py:237
  48.0 8.9 %all-gather.2.cloned.1.call-done = bf16[4,576,512]{2,1,0:T(8,128)(2,1)} async-done(((bf16[1,576,512]{2,1,0:T(8,128)(2,1)}), bf16[4,576,512]{2,1,0:T(8,128)(2,1)}) %all-gather.2.cloned.1.call-update) | async-done | bytes 2359312 | tf_op jit(solution)/shard_map/all_gather | solution.py:298
  56.9 1.9 %slice_bitcast_fusion.3 = (bf16[576,512]{1,0:T(8,128)(2,1)S(1)}, bf16[576,512]{1,0:T(8,128)(2,1)S(1)}, bf16[576,512]{1,0:T(8,128)(2,1)S(1)}, bf16[576,512]{1,0:T(8,128)(2,1)S(1)}) fusion(bf16[4,576,512]{2,1,0:T(8,128)(2,1)} %all-gather.2.cloned.1.call-done), kind=kLoop, calls=%fused_computation.35 | loop fusion | bytes 4718592 | tf_op jit(solution)/shard_map/squeeze | solution.py:299
  58.8 0.8 copy-done.3
  59.8 4.1 %fusion.4 = f32[576,1024]{1,0:T(8,128)} fusion(bf16[1,2048,1024]{2,1,0:T(8,128)(2,1)S(1)} %copy-done.13, bf16[576,512]{1,0:T(8,128)(2,1)S(1)} %get-tuple-element.5, bf16[576,512]{1,0:T(8,128)(2,1)S(1)} %get-tuple-element.6, bf16[576,512]{1,0:T(8,128)(2,1)S(1)} %get-tuple-element.7, bf16[576,512]{1,0:T(8,128)(2,1)S(1)} %get-tuple-element.4), kind=kOutput, calls=%fused_computation.4 | convolution fusion | flops 2425356288 | bytes 8912896 | tf_op jit(solution)/shard_map/dot_general | solution.py:300
  63.9 11.0 %fusion.6 = bf16[576,2048]{1,0:T(8,128)(2,1)} fusion(bf16[1,1024,2048]{2,1,0:T(8,128)(2,1)} %param.28, f32[576,1024]{1,0:T(8,128)} %fusion.4, bf16[1,2048,1024]{2,1,0:T(8,128)(2,1)} %param.27, bf16[576,512]{1,0:T(8,128)(2,1)S(1)} %get-tuple-element.5, bf16[576,512]{1,0:T(8,128)(2,1)} %copy-done.3, bf16[576,512]{1,0:T(8,128)(2,1)} %copy-done.4, ...), kind=kOutput, calls=%fused_computation.6 | convolution fusion | flops 4845993984 | bytes 15466496 | tf_op jit(solution)/shard_map/dot_general | solution.py:303
  75.0 25.9 %all-to-all-done = bf16[8,384,384]{2,1,0:T(8,128)(2,1)S(1)} async-done(((bf16[8,384,384]{2,1,0:T(8,128)(2,1)}), bf16[8,384,384]{2,1,0:T(8,128)(2,1)S(1)}, u32[]{:S(2)}, u32[]{:S(2)}) %all-to-all-start) | async-done | bytes 2359328 | tf_op jit(solution)/shard_map/all_to_all | solution.py:237
  100.9 1.4 copy-done.1
  102.3 27.9 %attend_send.1 = bf16[384,1024]{1,0:T(8,128)(2,1)} custom-call(bf16[3072,384]{1,0:T(8,128)(2,1)} %bitcast.55), custom_call_target="tpu_custom_call" | custom-call | flops 9663676416 | bytes 3145728 | tf_op jit(solution)/shard_map/attend_send/pallas_call | solution.py:159
  130.2 5.4 %convolution_convert_fusion = bf16[384,2048]{1,0:T(8,128)(2,1)} fusion(bf16[384,1024]{1,0:T(8,128)(2,1)} %attend_send.1, bf16[1024,2048]{1,0:T(8,128)(2,1)} %param.20), kind=kOutput, calls=%fused_computation.7 | convolution fusion | flops 1611399168 | bytes 6553600 | tf_op jit(solution)/shard_map/dot_general | solution.py:247
  135.7 6.0 %all-to-all-start.2 = ((bf16[8,72,512]{2,1,0:T(8,128)(2,1)}), bf16[8,72,512]{2,1,0:T(8,128)(2,1)S(1)}, u32[]{:S(2)}, u32[]{:S(2)}) async-start(bf16[8,72,512]{2,1,0:T(8,128)(2,1)} %bitcast.58), calls=%async_computation.4 | async-start | bytes 1179648 | tf_op jit(solution)/shard_map/all_to_all | solution.py:307
  141.7 23.5 %reduce-scatter.3.cloned.1.call-done = bf16[96,2048]{1,0:T(8,128)(2,1)} async-done(((bf16[384,2048]{1,0:T(8,128)(2,1)}), bf16[96,2048]{1,0:T(8,128)(2,1)}) %reduce-scatter.3.cloned.1.call-update) | async-done | bytes 393232 | tf_op jit(solution)/shard_map/reduce_scatter | solution.py:246
  165.2 1.2 fusion.16
  166.4 1.9 %fusion.18 = bf16[96,2048]{1,0:T(8,128)(2,1)} fusion(bf16[96,2048]{1,0:T(8,128)(2,1)} %reduce-scatter.3.cloned.1.call-done, f32[2048]{0:T(1024)S(1)} %copy-done.7, f32[96]{0:T(128)S(1)} %add_rsqrt_fusion.4), kind=kLoop, calls=%fused_computation.24 | loop fusion | flops 786432 | bytes 795008 | tf_op jit(solution)/shard_map/convert_element_type | solution.py:257
  168.3 0.4 convolution_multiply_fusion
  168.7 0.5 multiply_reduce_fusion.2
  169.1 5.8 %psum.7 = f32[192]{0:T(256)S(1)} all-reduce(f32[192]{0:T(256)S(1)} %get-tuple-element.32), channel_id=1, replica_groups=mesh['ep'=8,'tp'=4] {'tp'}, use_global_device_ids=true, to_apply=%region_9.10 | all-reduce | flops 192 | bytes 1536 | tf_op jit(solution)/shard_map/psum | solution.py:313
  174.9 0.8 multiply_convert_fusion.1
  (59 shorter events, 3.0 us)
Async XLA Ops:
  7.2 1.4 copy-start
  7.2 1.7 copy-start.8
  7.2 49.7 %all-gather.2.cloned.1.call-start = ((), (), s32[]{:S(2)}) async-start(), calls=%async_computation.6 | async-start | bytes 2949120 | tf_op jit(solution)/shard_map/all_gather | solution.py:298
  8.6 25.6 %copy-start.2 = (bf16[384,1024]{1,0:T(8,128)(2,1)S(1)}, bf16[384,1024]{1,0:T(8,128)(2,1)}, u32[]{:S(2)}) copy-start(bf16[384,1024]{1,0:T(8,128)(2,1)} %param.15) | copy-start | bytes 2359300
  10.3 25.3 %copy-start.6 = (bf16[384,512]{1,0:T(8,128)(2,1)S(1)}, bf16[384,512]{1,0:T(8,128)(2,1)}, u32[]{:S(2)}) copy-start(bf16[384,512]{1,0:T(8,128)(2,1)} %param.16) | copy-start | bytes 1179652
  34.2 2.2 %copy-start.11 = (f32[128]{0:T(128)S(1)}, f32[128]{0:T(128)}, u32[]{:S(2)}) copy-start(f32[128]{0:T(128)} %param.19) | copy-start | bytes 1540
  38.3 1.5 copy-start.5
  38.3 2.1 %copy-start.12 = (f32[128]{0:T(128)S(1)}, f32[128]{0:T(128)}, u32[]{:S(2)}) copy-start(f32[128]{0:T(128)} %param.18) | copy-start | bytes 1540
  44.1 56.7 %all-to-all-start = ((bf16[8,384,384]{2,1,0:T(8,128)(2,1)}), bf16[8,384,384]{2,1,0:T(8,128)(2,1)S(1)}, u32[]{:S(2)}, u32[]{:S(2)}) async-start(bf16[8,384,384]{2,1,0:T(8,128)(2,1)} %copy.67), calls=%async_computation | async-start | bytes 4718592 | tf_op jit(solution)/shard_map/all_to_all | solution.py:237
  47.7 87.9 %reduce-scatter.5.cloned.1.call-start = ((), (), s32[]{:S(2)}) async-start(), calls=%async_computation.7 | async-start | bytes 2949120 | tf_op jit(solution)/shard_map/reduce_scatter | solution.py:304
  56.9 3.0 %copy-start.13 = (bf16[1,2048,1024]{2,1,0:T(8,128)(2,1)S(1)}, bf16[1,2048,1024]{2,1,0:T(8,128)(2,1)}, u32[]{:S(2)}) copy-start(bf16[1,2048,1024]{2,1,0:T(8,128)(2,1)} %param.26) | copy-start | bytes 12582916
  58.8 0.8 copy-start.3
  58.8 1.0 copy-start.4
  75.0 90.2 %reduce-scatter.3.cloned.1.call-start = ((), (), s32[]{:S(2)}) async-start(), calls=%async_computation.5 | async-start | bytes 1966080 | tf_op jit(solution)/shard_map/reduce_scatter | solution.py:246
  100.9 1.4 copy-start.1
  135.6 6.0 %copy-start.10 = (f32[192,2]{0,1:T(2,128)S(1)}, f32[192,2]{0,1:T(2,128)}, u32[]{:S(2)}) copy-start(f32[192,2]{0,1:T(2,128)} %param.24) | copy-start | bytes 4612
  135.6 30.8 %copy-start.7 = (f32[2048]{0:T(1024)S(1)}, f32[2048]{0:T(1024)}, u32[]{:S(2)}) copy-start(f32[2048]{0:T(1024)} %param.21) | copy-start | bytes 24580
  135.7 39.2 %copy-start.9 = (f32[512]{0:T(512)S(1)}, f32[512]{0:T(512)}, u32[]{:S(2)}) copy-start(f32[512]{0:T(512)} %param.29) | copy-start | bytes 6148
  135.7 32.6 %all-to-all-start.2 = ((bf16[8,72,512]{2,1,0:T(8,128)(2,1)}), bf16[8,72,512]{2,1,0:T(8,128)(2,1)S(1)}, u32[]{:S(2)}, u32[]{:S(2)}) async-start(bf16[8,72,512]{2,1,0:T(8,128)(2,1)} %bitcast.58), calls=%async_computation.4 | async-start | bytes 1179648 | tf_op jit(solution)/shard_map/all_to_all | solution.py:307
Sparse Core Ops, SparseCore 0:
  34.3 22.4 all-gather.1
  75.1 32.7 reduce-scatter.4
  135.8 29.3 reduce-scatter.2
where the time goes:
time: 183 us; the launch traced here: 182 us
  waiting for transfers between devices  58.3 us (32%)
  blocking collectives  29.6 us (16%)
  Pallas kernels  27.9 us (15%)
  matrix products  21.7 us (12%)
  between operations  14.1 us (8%)
  other arithmetic  10.8 us (6%)
  starting transfers between devices  9.87 us (5%)
  local copies, waits for them, and re-layouts  9.83 us (5%)
    pallas_call x1, Pallas kernels, attend_send(): pl.pallas_call(functools.partial(attend_send_kernel, n_ep, head_dim ** (-...  27.9 us
    all_to_all x1, waiting for transfers between devices, mixer_half(): lax.all_to_all(outgoing, 'ep', split_axis=0, concat_axis=0, tiled=True)  25.9 us
    all_to_all x1, blocking collectives, expert_half(): lax.all_to_all(outgoing.reshape(expert_total, capacity, share), 'ep', spl...  23.8 us
    reduce_scatter x1, waiting for transfers between devices, mixer_half(): lax.psum_scatter(jnp.dot(attended, w_out, preferred_element_type=jnp.floa...  23.5 us
    dot_general x1, matrix products, expert_half(): jnp.dot(hidden, w_down[0], preferred_element_type=jnp.float32)  11 us
    all_gather x1, waiting for transfers between devices, expert_half(): shares = lax.all_gather(arrived, 'tp', axis=0, tiled=False)  8.87 us
    all_to_all x1, starting transfers between devices, expert_half(): lax.all_to_all(summed, 'ep', split_axis=0, concat_axis=0, tiled=True)  5.96 us
    psum x1, blocking collectives, expert_half(): squares = lax.psum(jnp.sum(combined * combined, axis=1), 'tp')  5.76 us
  transfers between devices with their start and end apart: 5, of which 3 were waited for; matrix products, arithmetic and copies ran while one was open for 19% of the time, Pallas kernels for 15%

commit v1 on v0

--- a/solution.py
+++ b/solution.py
@@ -315,6 +315,715 @@
     return scaled.astype(jnp.bfloat16)
 
 
+MESH_ID = pl.DeviceIdType.MESH
+KEY_STEP = 768
+FF_STEP = 256
+
+
+def remote(src, dst, send_sem, recv_sem, ep, tp):
+    return pltpu.make_async_remote_copy(
+        src_ref=src,
+        dst_ref=dst,
+        send_sem=send_sem,
+        recv_sem=recv_sem,
+        device_id={"ep": ep, "tp": tp},
+        device_id_type=MESH_ID,
+    )
+
+
+def aligned(index, size):
+    return pl.ds(pl.multiple_of(index * size, size), size)
+
+
+def turn_rows(raw, gain, cosine, sine, low_lane):
+    rows = raw.astype(jnp.float32)
+    mean = jnp.mean(rows * rows, axis=1, keepdims=True)
+    rows = rows * lax.rsqrt(mean + EPS) * gain
+    head_dim = rows.shape[1]
+    quarter = head_dim // 4
+    swapped = jnp.where(
+        low_lane, pltpu.roll(rows, head_dim - quarter, 1), pltpu.roll(rows, quarter, 1)
+    )
+    return (rows * cosine + swapped * sine).astype(jnp.bfloat16)
+
+
+def attend_heads(query, k_ref, vt_ref, first_done):
+    columns, head_dim = query.shape
+    steps = k_ref.shape[0] // KEY_STEP
+    top = jnp.full((1, columns), -1e30, jnp.float32)
+    total = jnp.zeros((1, columns), jnp.float32)
+    acc = jnp.zeros((head_dim, columns), jnp.float32)
+    for index in range(steps):
+        rows = slice(index * KEY_STEP, (index + 1) * KEY_STEP)
+        scores = lax.dot_general(
+            k_ref[rows, :], query, (((1,), (1,)), ((), ())), preferred_element_type=jnp.float32
+        )
+        new_top = jnp.maximum(top, jnp.max(scores, axis=0, keepdims=True))
+        exponent = jnp.exp2(scores - new_top)
+        factor = jnp.exp2(top - new_top)
+        total = total * factor + jnp.sum(exponent, axis=0, keepdims=True)
+        acc = acc * factor + jnp.dot(
+            vt_ref[:, rows], exponent.astype(jnp.bfloat16), preferred_element_type=jnp.float32
+        )
+        top = new_top
+    return (acc / total).T.astype(jnp.bfloat16)
+
+
+def layer_kernel(
+    n_z,
+    n_x,
+    n_tp,
+    cap,
+    q_ref,
+    k_ref,
+    v_ref,
+    cos_ref,
+    sin_ref,
+    q_gain,
+    k_gain,
+    mixer_gain,
+    x_ref,
+    ids_ref,
+    weight_ref,
+    in_gain,
+    out_gain,
+    w_gate,
+    w_up,
+    w_down,
+    w_out,
+    mixer_out,
+    moe_out,
+    wg,
+    wu,
+    wd,
+    wo,
+    q_stage,
+    k_stage,
+    v_stage,
+    k_all,
+    vt_all,
+    q_all,
+    o_stage,
+    o_all,
+    picker,
+    x_stage,
+    x_all,
+    hidden,
+    part_send,
+    part_keep,
+    part_recv,
+    pair_send,
+    pair_recv,
+    rows_out,
+    returned,
+    squares_send,
+    squares_recv,
+    head_send,
+    head_keep,
+    head_recv,
+    head_pair,
+    head_last,
+    w_sem,
+    own_sem,
+    mz_s,
+    mz_r,
+    mx_s,
+    mx_r,
+    my_s,
+    my_r,
+    mc_s,
+    mc_r,
+    k_s,
+    k_r,
+    vz_s,
+    vz_r,
+    kx_s,
+    kx_r,
+    vx_s,
+    vx_r,
+    q_s,
+    q_r,
+    o_s,
+    o_r,
+    pc_s,
+    pc_r,
+    py_s,
+    py_r,
+    ret_s,
+    ret_r,
+    sq_s,
+    sq_r,
+    hc_s,
+    hc_r,
+    hy_s,
+    hy_r,
+):
+    me = lax.axis_index("ep")
+    t = lax.axis_index("tp")
+    z = me // n_x
+    x = lax.rem(me, n_x)
+    other_x = 1 - x
+    core = t + 1 - 2 * lax.rem(t, 2)
+    across = lax.rem(t + 2, n_tp)
+    diagonal = lax.rem(core + 2, n_tp)
+    x_peer = z * n_x + other_x
+
+    def plane(offset):
+        return lax.rem(z + offset, n_z)
+
+    def source(offset):
+        return lax.rem(z + n_z - offset, n_z)
+
+    weights = [
+        pltpu.make_async_copy(w_gate.at[0], wg, w_sem.at[0]),
+        pltpu.make_async_copy(w_up.at[0], wu, w_sem.at[1]),
+        pltpu.make_async_copy(w_down.at[0], wd, w_sem.at[2]),
+        pltpu.make_async_copy(w_out, wo, w_sem.at[3]),
+    ]
+    for copy in weights:
+        copy.start()
+
+    barrier = pltpu.get_barrier_semaphore()
+    greeted = [(plane(o) * n_x + x, t) for o in range(1, n_z)]
+    greeted += [(plane(o) * n_x + other_x, t) for o in range(n_z)]
+    greeted += [(me, core), (me, across), (me, diagonal)]
+    for ep, tp in greeted:
+        pl.semaphore_signal(barrier, inc=1, device_id={"ep": ep, "tp": tp}, device_id_type=MESH_ID)
+
+    rows, width = x_ref.shape
+    share = width // n_tp
+    own_cols = aligned(t, share)
+    group_rows = n_z * cap
+    x_full = x_ref[...].astype(jnp.float32)
+    scale = lax.rsqrt(jnp.mean(x_full * x_full, axis=1, keepdims=True) + EPS)
+    normed = (x_ref[:, own_cols].astype(jnp.float32) * scale * in_gain[:, own_cols]).astype(
+        jnp.bfloat16
+    )
+    first_id = ids_ref[:, 0:1]
+    lane = lax.broadcasted_iota(jnp.int32, (rows, 128), 1)
+    in_group = (first_id >= lane * n_x) & (first_id < lane * n_x + n_x)
+    row_at = lax.broadcasted_iota(jnp.int32, (rows, rows), 0)
+    col_at = lax.broadcasted_iota(jnp.int32, (rows, rows), 1)
+    earlier = jnp.where(col_at < row_at, 1.0, 0.0).astype(jnp.bfloat16)
+    counts = jnp.dot(
+        earlier,
+        jnp.where(in_group, 1.0, 0.0).astype(jnp.bfloat16),
+        preferred_element_type=jnp.float32,
+    )
+    slot = jnp.sum(
+        jnp.where(in_group, counts + (lane * cap).astype(jnp.float32), 0.0), axis=1, keepdims=True
+    )
+    slot_at = lax.broadcasted_iota(jnp.int32, (rows, group_rows), 1).astype(jnp.float32)
+    picker[...] = jnp.where(slot_at == slot, 1.0, 0.0).astype(jnp.bfloat16)
+    x_stage[...] = lax.dot_general(
+        picker[...], normed, (((0,), (0,)), ((), ())), preferred_element_type=jnp.float32
+    ).astype(jnp.bfloat16)
+    pl.semaphore_wait(barrier, len(greeted))
+
+    def chunk_at(region, index):
+        return x_all.at[region, aligned(index, cap), own_cols]
+
+    sent = []
+
+    def go(copy):
+        copy.start()
+        sent.append(copy)
+        return copy
+
+    own_rows = x_stage.at[aligned(z, cap), :]
+    moe_z = []
+    for o in (2, 1, 3):
+        moe_z.append(
+            go(
+                remote(
+                    x_stage.at[aligned(plane(o), cap), :],
+                    chunk_at(0, z),
+                    mz_s.at[o - 1],
+                    mz_r.at[o - 1],
+                    plane(o) * n_x + x,
+                    t,
+                )
+            )
+        )
+    own_x = pltpu.make_async_copy(own_rows, chunk_at(0, z), own_sem.at[0])
+    own_x.start()
+    moe_x = [go(remote(own_rows, chunk_at(1, z), mx_s.at[0], mx_r.at[0], x_peer, t))]
+    moe_y = [[go(remote(own_rows, chunk_at(0, z), my_s.at[0, 0], my_r.at[0, 0], me, across))], []]
+
+    tokens, kv_width = k_ref.shape
+    head_dim = q_gain.shape[1]
+    q_width = q_ref.shape[1] // n_z
+    lanes = lax.broadcasted_iota(jnp.int32, (tokens, head_dim), 1)
+    low_lane = lax.rem(lanes, head_dim // 2) < head_dim // 4
+    cosine, sine = cos_ref[...], sin_ref[...]
+    for g in range(n_z):
+        cols = slice(g * head_dim, (g + 1) * head_dim)
+        k_stage[g] = turn_rows(k_ref[:, cols], k_gain[...], cosine, sine, low_lane)
+        v_stage[g] = v_ref[:, cols].T
+
+    def k_at(region, index):
+        return k_all.at[aligned(region * n_z + index, tokens), :]
+
+    def v_at(region, index):
+        return vt_all.at[:, aligned(region * n_z + index, tokens)]
+
+    kv_z = []
+    for o in (2, 1, 3):
+        to = plane(o)
+        kv_z.append(
+            (
+                go(remote(k_stage.at[to], k_at(0, z), k_s.at[o - 1], k_r.at[o - 1], to * n_x + x, t)),
+                go(
+                    remote(
+                        v_stage.at[to], v_at(0, z), vz_s.at[o - 1], vz_r.at[o - 1], to * n_x + x, t
+                    )
+                ),
+            )
+        )
+    own_k = pltpu.make_async_copy(k_stage.at[z], k_at(0, z), own_sem.at[1])
+    own_v = pltpu.make_async_copy(v_stage.at[z], v_at(0, z), own_sem.at[2])
+    own_k.start()
+    own_v.start()
+    kv_x = [
+        go(remote(k_stage.at[z], k_at(1, z), kx_s.at[0], kx_r.at[0], x_peer, t)),
+        go(remote(v_stage.at[z], v_at(1, z), vx_s.at[0], vx_r.at[0], x_peer, t)),
+    ]
+
+    heads = q_width // head_dim
+    to_exponent = head_dim**-0.5 * math.log2(math.e)
+    for g in range(n_z):
+        for h in range(heads):
+            cols = slice((g * heads + h) * head_dim, (g * heads + h + 1) * head_dim)
+            q_stage[g, :, h * head_dim : (h + 1) * head_dim] = turn_rows(
+                q_ref[:, cols], q_gain[...] * to_exponent, cosine, sine, low_lane
+            )
+    for o in (1, 2, 3):
+        to = plane(o)
+        go(remote(q_stage.at[to], q_all.at[z], q_s.at[o - 1], q_r.at[o - 1], to * n_x + x, t))
+    own_q = pltpu.make_async_copy(q_stage.at[z], q_all.at[z], own_sem.at[3])
+    own_q.start()
+
+    for copy, o in zip(moe_z, (2, 1, 3)):
+        copy.wait_recv()
+        here = chunk_at(0, source(o))
+        moe_y[0].append(go(remote(here, here, my_s.at[0, o], my_r.at[0, o], me, across)))
+        moe_x.append(
+            go(remote(here, chunk_at(1, source(o)), mx_s.at[o], mx_r.at[o], x_peer, t))
+        )
+    own_x.wait()
+
+    def cols_at(region, tp):
+        return x_all.at[region, :, aligned(tp, share)]
+
+    moe_c = [[], []]
+    moe_c[0].append(
+        go(remote(cols_at(0, t), cols_at(0, t), mc_s.at[0, 0], mc_r.at[0, 0], me, core))
+    )
+    for copy, o in zip(moe_x, (0, 2, 1, 3)):
+        copy.wait_recv()
+        here = chunk_at(1, source(o))
+        moe_y[1].append(go(remote(here, here, my_s.at[1, o], my_r.at[1, o], me, across)))
+    moe_c[1].append(
+        go(remote(cols_at(1, t), cols_at(1, t), mc_s.at[1, 0], mc_r.at[1, 0], me, core))
+    )
+    for copy in moe_y[0]:
+        copy.wait_recv()
+    moe_c[0].append(
+        go(remote(cols_at(0, across), cols_at(0, across), mc_s.at[0, 1], mc_r.at[0, 1], me, core))
+    )
+
+    def forward_keys(index, o):
+        key_copy, value_copy = kv_z[index]
+        key_copy.wait_recv()
+        kv_x.append(
+            go(
+                remote(
+                    k_at(0, source(o)), k_at(1, source(o)), kx_s.at[o], kx_r.at[o], x_peer, t
+                )
+            )
+        )
+        value_copy.wait_recv()
+        kv_x.append(
+            go(
+                remote(
+                    v_at(0, source(o)), v_at(1, source(o)), vx_s.at[o], vx_r.at[o], x_peer, t
+                )
+            )
+        )
+
+    blocks = (core, diagonal, t, across)
+    inner_width = wg.shape[1]
+
+    def experts(region):
+        for copy in moe_c[region]:
+            copy.wait_recv()
+        if region == 0:
+            weights[0].wait()
+            weights[1].wait()
+
+        def pre(index, carry):
+            cols = aligned(index, FF_STEP)
+            rows_in = x_all[region]
+            gate = jnp.dot(rows_in, wg[:, cols], preferred_element_type=jnp.float32)
+            up = jnp.dot(rows_in, wu[:, cols], preferred_element_type=jnp.float32)
+            hidden[:, cols] = (gate / (1.0 + jnp.exp(-gate)) * up).astype(jnp.bfloat16)
+            return carry
+
+        lax.fori_loop(0, inner_width // FF_STEP, pre, 0)
+        if region == 0:
+            weights[2].wait()
+        for index, block in enumerate(blocks):
+            part = jnp.dot(
+                hidden[...], wd[:, aligned(block, share)], preferred_element_type=jnp.float32
+            ).astype(jnp.bfloat16)
+            if index < 2:
+                part_send[region, index] = part
+                go(
+                    remote(
+                        part_send.at[region, index],
+                        part_recv.at[region, index],
+                        pc_s.at[region, index],
+                        pc_r.at[region, index],
+                        me,
+                        core,
+                    )
+                )
+            else:
+                part_keep[region, index - 2] = part
+
+    def part_copy(region, index):
+        return remote(
+            part_send.at[region, index],
+            part_recv.at[region, index],
+            pc_s.at[region, index],
+            pc_r.at[region, index],
+            me,
+            core,
+        )
+
+    def pair_copy(region):
+        return remote(
+            pair_send.at[region], pair_recv.at[region], py_s.at[region], py_r.at[region], me, across
+        )
+
+    def pair(region):
+        part_copy(region, 1).wait_recv()
+        pair_send[region] = (
+            part_keep[region, 1].astype(jnp.float32) + part_recv[region, 1].astype(jnp.float32)
+        ).astype(jnp.bfloat16)
+        sent.append(pair_copy(region))
+        sent[-1].start()
+
+    experts(0)
+    pair(0)
+    forward_keys(0, 2)
+    forward_keys(1, 1)
+    for copy in moe_y[1]:
+        copy.wait_recv()
+    moe_c[1].append(
+        go(remote(cols_at(1, across), cols_at(1, across), mc_s.at[1, 1], mc_r.at[1, 1], me, core))
+    )
+    forward_keys(2, 3)
+    experts(1)
+    pair(1)
+
+    def return_copy(region, o):
+        to = plane(o)
+        return remote(
+            rows_out.at[region, aligned(to, cap), :],
+            returned.at[aligned(x * n_z + z, cap), :],
+            ret_s.at[region, o],
+            ret_r.at[region, o],
+            to * n_x + (x if region == 0 else other_x),
+            t,
+        )
+
+    own_return = pltpu.make_async_copy(
+        rows_out.at[0, aligned(z, cap), :],
+        returned.at[aligned(x * n_z + z, cap), :],
+        own_sem.at[4],
+    )
+    returns = [(0, o) for o in range(1, n_z)] + [(1, o) for o in range(n_z)]
+
+    def send_back():
+        for region in range(n_x):
+            part_copy(region, 0).wait_recv()
+            pair_copy(region).wait_recv()
+            rows_out[region] = (
+                part_keep[region, 0].astype(jnp.float32)
+                + part_recv[region, 0].astype(jnp.float32)
+                + pair_recv[region].astype(jnp.float32)
+            ).astype(jnp.bfloat16)
+        for region, o in returns:
+            return_copy(region, o).start()
+        own_return.start()
+
+    for copy in kv_x:
+        copy.wait_recv()
+    own_k.wait()
+    own_v.wait()
+    own_q.wait()
+
+    def output_copy(o):
+        to = plane(o)
+        return remote(
+            o_stage.at[to],
+            o_all.at[:, aligned(z, q_width)],
+            o_s.at[o - 1],
+            o_r.at[o - 1],
+            to * n_x + x,
+            t,
+        )
+
+    def block(index, carry):
+        o = index + 1
+        to = plane(o)
+
+        @pl.when(o < n_z)
+        def _():
+            back = n_z - o
+            remote(
+                q_stage.at[to], q_all.at[to], q_s.at[back - 1], q_r.at[back - 1], me, core
+            ).wait_recv()
+
+        for h in range(heads):
+            cols = slice(h * head_dim, (h + 1) * head_dim)
+            o_stage[to, :, cols] = attend_heads(q_all[to, :, cols], k_all, vt_all, None)
+
+        @pl.when(o < n_z)
+        def _():
+            output_copy(o).start()
+
+        @pl.when(o == n_z // 2)
+        def _():
+            send_back()
+
+        return carry
+
+    lax.fori_loop(0, n_z, block, 0)
+    own_o = pltpu.make_async_copy(
+        o_stage.at[z], o_all.at[:, aligned(z, q_width)], own_sem.at[5]
+    )
+    own_o.start()
+    weights[3].wait()
+    for o in range(1, n_z):
+        output_copy(o).wait_recv()
+    own_o.wait()
+
+    own_tokens = tokens // n_tp
+    out_width = wo.shape[1]
+
+    def project(first, second, into):
+        taken = jnp.concatenate(
+            [o_all[aligned(first, own_tokens), :], o_all[aligned(second, own_tokens), :]], axis=0
+        )
+
+        def columns(index, carry):
+            cols = aligned(index, 512)
+            part = jnp.dot(taken, wo[:, cols], preferred_element_type=jnp.float32).astype(
+                jnp.bfloat16
+            )
+            into[0, :, cols] = part[:own_tokens]
+            into[1, :, cols] = part[own_tokens:]
+            return carry
+
+        lax.fori_loop(0, out_width // 512, columns, 0)
+
+    project(core, diagonal, head_send)
+    head_c = [
+        go(remote(head_send.at[i], head_recv.at[i], hc_s.at[i], hc_r.at[i], me, core))
+        for i in (1, 0)
+    ]
+    project(t, across, head_keep)
+    head_c[0].wait_recv()
+    head_pair[...] = (
+        head_keep[1].astype(jnp.float32) + head_recv[1].astype(jnp.float32)
+    ).astype(jnp.bfloat16)
+    head_y = go(remote(head_pair, head_last, hy_s.at[0], hy_r.at[0], me, across))
+
+    for region, o in returns:
+        return_copy(region, o).wait_recv()
+    own_return.wait()
+    picks = picker[...]
+    ids = ids_ref[...]
+    mix = weight_ref[...]
+    combined = jnp.zeros((rows, share), jnp.float32)
+    for parity in range(n_x):
+        gathered = jnp.dot(
+            picks,
+            returned[parity * group_rows : (parity + 1) * group_rows, :],
+            preferred_element_type=jnp.float32,
+        )
+        factor = jnp.sum(
+            jnp.where(lax.rem(ids, n_x) == parity, mix, 0.0), axis=1, keepdims=True
+        )
+        combined = combined + gathered * factor
+    squares = jnp.sum(combined * combined, axis=1, keepdims=True)
+    squares_send[...] = jnp.broadcast_to(squares, (rows, 128)).T[0:8, :]
+    square_copies = [
+        go(remote(squares_send, squares_recv.at[i], sq_s.at[i], sq_r.at[i], me, tp))
+        for i, tp in enumerate((core, across, diagonal))
+    ]
+    for copy in square_copies:
+        copy.wait_recv()
+    all_squares = squares_send[...] + squares_recv[0] + squares_recv[1] + squares_recv[2]
+    spread = jnp.broadcast_to(all_squares[0:1, :], (128, rows)).T[:, 0:1]
+    moe_out[...] = (combined * lax.rsqrt(spread / width + EPS) * out_gain[...]).astype(
+        jnp.bfloat16
+    )
+
+    head_c[1].wait_recv()
+    head_y.wait_recv()
+    mixed = (
+        head_keep[0].astype(jnp.float32)
+        + head_recv[0].astype(jnp.float32)
+        + head_last[...].astype(jnp.float32)
+    )
+    mean = jnp.mean(mixed * mixed, axis=1, keepdims=True)
+    mixer_out[...] = (mixed * lax.rsqrt(mean + EPS) * mixer_gain[...]).astype(jnp.bfloat16)
+
+    for copy in sent:
+        copy.wait_send()
+    for o in range(1, n_z):
+        output_copy(o).wait_send()
+    for region, o in returns:
+        return_copy(region, o).wait_send()
+
+
+def turn_tables(row_count, row_offset, head_dim):
+    position = row_offset + jnp.arange(row_count, dtype=jnp.int32)
+    half_width = head_dim // 2
+    frequency = THETA ** (-jnp.arange(0, half_width, 2, dtype=jnp.float32) / half_width)
+    row_angle = (position // GRID).astype(jnp.float32)[:, None] * frequency[None, :]
+    col_angle = (position % GRID).astype(jnp.float32)[:, None] * frequency[None, :]
+    angles = jnp.concatenate([row_angle, row_angle, col_angle, col_angle], axis=1)
+    lane = jnp.arange(head_dim, dtype=jnp.int32)[None, :]
+    sign = jnp.where(lane % half_width < half_width // 2, -1.0, 1.0)
+    return jnp.cos(angles), jnp.sin(angles) * sign
+
+
+def layer(
+    n_z,
+    n_x,
+    query_rows,
+    key_rows,
+    value_rows,
+    query_gain,
+    key_gain,
+    w_out,
+    mixer_gain,
+    expert_input,
+    expert_ids,
+    expert_weights,
+    input_gain,
+    w_gate,
+    w_up,
+    w_down,
+    out_gain,
+):
+    n_tp = lax.axis_size("tp")
+    tokens = query_rows.shape[0]
+    head_dim = query_gain.shape[0]
+    rows, width = expert_input.shape
+    share = width // n_tp
+    inner = w_gate.shape[2]
+    q_width = query_rows.shape[1] // n_z
+    cap = -(-(3 * rows // (4 * n_x)) // 16) * 16
+    cosine, sine = turn_tables(tokens, lax.axis_index("ep") * tokens, head_dim)
+    bf16, f32 = jnp.bfloat16, jnp.float32
+    vmem = pl.BlockSpec(memory_space=pltpu.VMEM)
+    hbm = pl.BlockSpec(memory_space=pl.ANY)
+    dma = pltpu.SemaphoreType.DMA
+    group_rows = n_z * cap
+    own_tokens = tokens // n_tp
+    far = n_z - 1
+    scratch = [
+        pltpu.VMEM(w_gate.shape[1:], bf16),
+        pltpu.VMEM(w_up.shape[1:], bf16),
+        pltpu.VMEM(w_down.shape[1:], bf16),
+        pltpu.VMEM(w_out.shape, bf16),
+        pltpu.VMEM((n_z, tokens, q_width), bf16),
+        pltpu.VMEM((n_z, tokens, head_dim), bf16),
+        pltpu.VMEM((n_z, head_dim, tokens), bf16),
+        pltpu.VMEM((n_x * n_z * tokens, head_dim), bf16),
+        pltpu.VMEM((head_dim, n_x * n_z * tokens), bf16),
+        pltpu.VMEM((n_z, tokens, q_width), bf16),
+        pltpu.VMEM((n_z, tokens, q_width), bf16),
+        pltpu.VMEM((tokens, n_z * q_width), bf16),
+        pltpu.VMEM((rows, group_rows), bf16),
+        pltpu.VMEM((group_rows, share), bf16),
+        pltpu.VMEM((n_x, group_rows, width), bf16),
+        pltpu.VMEM((group_rows, inner), bf16),
+        pltpu.VMEM((n_x, 2, group_rows, share), bf16),
+        pltpu.VMEM((n_x, 2, group_rows, share), bf16),
+        pltpu.VMEM((n_x, 2, group_rows, share), bf16),
+        pltpu.VMEM((n_x, group_rows, share), bf16),
+        pltpu.VMEM((n_x, group_rows, share), bf16),
+        pltpu.VMEM((n_x, group_rows, share), bf16),
+        pltpu.VMEM((n_x * group_rows, share), bf16),
+        pltpu.VMEM((8, rows), f32),
+        pltpu.VMEM((3, 8, rows), f32),
+        pltpu.VMEM((2, own_tokens, width), bf16),
+        pltpu.VMEM((2, own_tokens, width), bf16),
+        pltpu.VMEM((2, own_tokens, width), bf16),
+        pltpu.VMEM((own_tokens, width), bf16),
+        pltpu.VMEM((own_tokens, width), bf16),
+        dma((4,)),
+        dma((6,)),
+    ]
+    for shape in (
+        (far,),
+        (n_z,),
+        (n_x, n_z),
+        (n_x, 2),
+        (far,),
+        (far,),
+        (n_z,),
+        (n_z,),
+        (far,),
+        (far,),
+        (n_x, 2),
+        (n_x,),
+        (n_x, n_z),
+        (3,),
+        (2,),
+        (1,),
+    ):
+        scratch += [dma(shape), dma(shape)]
+    return pl.pallas_call(
+        functools.partial(layer_kernel, n_z, n_x, n_tp, cap),
+        in_specs=[vmem] * 13 + [hbm] * 4,
+        out_specs=(vmem, vmem),
+        out_shape=(
+            jax.ShapeDtypeStruct((own_tokens, width), bf16),
+            jax.ShapeDtypeStruct((rows, share), bf16),
+        ),
+        scratch_shapes=scratch,
+        compiler_params=pltpu.CompilerParams(
+            collective_id=0, has_side_effects=True, vmem_limit_bytes=60 * 1024 * 1024
+        ),
+        name="layer",
+    )(
+        query_rows,
+        key_rows,
+        value_rows,
+        cosine,
+        sine,
+        query_gain[None, :],
+        key_gain[None, :],
+        mixer_gain[None, :],
+        expert_input,
+        expert_ids,
+        expert_weights,
+        input_gain[None, :],
+        out_gain[None, :],
+        w_gate,
+        w_up,
+        w_down,
+        w_out,
+    )
+
+
 def per_device(
     query_rows,
     key_rows,
@@ -332,6 +1041,36 @@
     w_down,
     out_gain,
 ):
+    n_ep = lax.axis_size("ep")
+    n_z = key_rows.shape[1] // query_gain.shape[0]
+    n_x = w_gate.shape[0] * n_ep // GROUPS
+    if (
+        n_z == GROUPS
+        and n_z * n_x == n_ep
+        and n_x == 2
+        and expert_ids.shape[1] == n_x
+        and w_gate.shape[0] == 1
+        and lax.axis_size("tp") == 4
+    ):
+        return layer(
+            n_z,
+            n_x,
+            query_rows,
+            key_rows,
+            value_rows,
+            query_gain,
+            key_gain,
+            w_out,
+            mixer_gain,
+            expert_input,
+            expert_ids,
+            expert_weights,
+            input_gain,
+            w_gate,
+            w_up,
+            w_down,
+            out_gain,
+        )
     mixer_result = mixer_half(
         query_rows, key_rows, value_rows, query_gain, key_gain, w_out, mixer_gain
     )

time: 183 us -> 108 us (0.59)
  the two profiles are of different devices: /device:TPU:0 before, /device:TPU:9 now
where the time goes in v1:
time: 108 us
  Pallas kernels  99.1 us (92%)
  local copies, waits for them, and re-layouts  6.26 us (6%)
  other arithmetic  1.75 us (2%)
    pallas_call x1, Pallas kernels, layer(): pl.pallas_call(functools.partial(layer_kernel, n_z, n_x, n_tp, cap), in_s...  99.1 us
    unnamed x4, local copies, waits for them, and re-layouts  6.26 us

profile of v1, /device:TPU:9, one launch (start us, length us, event | category | flops | bytes accessed | tf_op | source)
XLA Modules:
  0.0 107.8 jit_solution(6045109154168321957)
XLA Ops:
  0.7 1.4 %copy.17.ids_ref = s32[192,2]{1,0:T(8,128)} copy(s32[192,2]{0,1:T(2,128)} %param.23) | data formatting | bytes 3072 | tf_op args[8]
  2.1 1.4 %copy.18.weight_ref = f32[192,2]{1,0:T(8,128)} copy(f32[192,2]{0,1:T(2,128)} %param.24) | data formatting | bytes 3072 | tf_op args[9]
  3.6 0.2 broadcast_multiply_fusion.1
  3.7 1.6 %sine_multiply_fusion = (f32[384,128]{1,0:T(8,128)}, f32[384,128]{1,0:T(8,128)}) fusion(f32[128]{0:T(128)S(1)} %compare_select_fusion, f32[384,32]{1,0:T(8,128)S(1)} %get-tuple-element.5, f32[384,32]{1,0:T(8,128)S(1)} %get-tuple-element.4), kind=kLoop, calls=%fused_computation.1 | loop fusion | flops 196608 | bytes 492032 | tf_op jit(solution)/shard_map/mul | solution.py:902
  5.3 99.1 %layer.1 = (bf16[96,2048]{1,0:T(8,128)(2,1)}, bf16[192,512]{1,0:T(8,128)(2,1)}) custom-call(bf16[384,1024]{1,0:T(8,128)(2,1)} %q_ref.1, bf16[384,512]{1,0:T(8,128)(2,1)} %k_ref.1, bf16[384,512]{1,0:T(8,128)(2,1)} %v_ref.1, f32[384,128]{1,0:T(8,128)} %get-tuple-element.3.cos_ref, f32[384,128]{1,0:T(8,128)} %get-tuple-element.2.sin_ref, f32[1,128]{1,0:T(1,128)} %bitcast.8, ...), custom_call_target="tpu_custom_call" | custom-call | tf_op jit(solution)/shard_map/layer/pallas_call | solution.py:993
  104.4 1.8 %copy.21 = bf16[96,2048]{1,0:T(8,128)(2,1)} copy(bf16[96,2048]{1,0:T(8,128)(2,1)} %get-tuple-element.10) | data formatting | bytes 786432
  106.1 1.6 %copy.22 = bf16[192,512]{1,0:T(8,128)(2,1)} copy(bf16[192,512]{1,0:T(8,128)(2,1)} %get-tuple-element.11) | data formatting | bytes 393216
  (3 shorter events, 0.0 us)

commit v2 on v1

--- a/solution.py
+++ b/solution.py
@@ -3,6 +3,7 @@
 
 import jax
 import jax.numpy as jnp
+import numpy as np
 from jax import lax
 from jax.experimental import pallas as pl
 from jax.experimental.pallas import tpu as pltpu
@@ -316,7 +317,6 @@
 
 
 MESH_ID = pl.DeviceIdType.MESH
-KEY_STEP = 768
 FF_STEP = 256
 
 
@@ -347,38 +347,31 @@
     return (rows * cosine + swapped * sine).astype(jnp.bfloat16)
 
 
-def attend_heads(query, k_ref, vt_ref, first_done):
-    columns, head_dim = query.shape
-    steps = k_ref.shape[0] // KEY_STEP
-    top = jnp.full((1, columns), -1e30, jnp.float32)
-    total = jnp.zeros((1, columns), jnp.float32)
-    acc = jnp.zeros((head_dim, columns), jnp.float32)
-    for index in range(steps):
-        rows = slice(index * KEY_STEP, (index + 1) * KEY_STEP)
-        scores = lax.dot_general(
-            k_ref[rows, :], query, (((1,), (1,)), ((), ())), preferred_element_type=jnp.float32
-        )
-        new_top = jnp.maximum(top, jnp.max(scores, axis=0, keepdims=True))
-        exponent = jnp.exp2(scores - new_top)
-        factor = jnp.exp2(top - new_top)
-        total = total * factor + jnp.sum(exponent, axis=0, keepdims=True)
-        acc = acc * factor + jnp.dot(
-            vt_ref[:, rows], exponent.astype(jnp.bfloat16), preferred_element_type=jnp.float32
-        )
-        top = new_top
-    return (acc / total).T.astype(jnp.bfloat16)
+def attend_keys(query, keys, values_t, state):
+    top, total, acc = state
+    scores = lax.dot_general(
+        keys, query, (((1,), (1,)), ((), ())), preferred_element_type=jnp.float32
+    )
+    new_top = jnp.maximum(top, jnp.max(scores, axis=0, keepdims=True))
+    exponent = jnp.exp2(scores - new_top)
+    factor = jnp.exp2(top - new_top)
+    total = total * factor + jnp.sum(exponent, axis=0, keepdims=True)
+    acc = acc * factor + jnp.dot(
+        values_t, exponent.astype(jnp.bfloat16), preferred_element_type=jnp.float32
+    )
+    return new_top, total, acc
 
 
 def layer_kernel(
-    n_z,
+    n_ep,
     n_x,
     n_tp,
     cap,
     q_ref,
     k_ref,
     v_ref,
-    cos_ref,
-    sin_ref,
+    row_table,
+    col_table,
     q_gain,
     k_gain,
     mixer_gain,
@@ -403,11 +396,16 @@
     k_all,
     vt_all,
     q_all,
+    tops,
+    totals,
+    accs,
     o_stage,
     o_all,
     picker,
     x_stage,
     x_all,
+    mix_stage,
+    mix_all,
     hidden,
     part_send,
     part_keep,
@@ -415,11 +413,12 @@
     pair_send,
     pair_recv,
     rows_out,
+    rows_in,
+    joined,
     returned,
     squares_send,
     squares_recv,
-    head_send,
-    head_keep,
+    head_part,
     head_recv,
     head_pair,
     head_last,
@@ -427,6 +426,8 @@
     own_sem,
     mz_s,
     mz_r,
+    mw_s,
+    mw_r,
     mx_s,
     mx_r,
     my_s,
@@ -435,12 +436,12 @@
     mc_r,
     k_s,
     k_r,
-    vz_s,
-    vz_r,
-    kx_s,
-    kx_r,
-    vx_s,
-    vx_r,
+    v_s,
+    v_r,
+    kf_s,
+    kf_r,
+    vf_s,
+    vf_r,
     q_s,
     q_r,
     o_s,
@@ -449,6 +450,8 @@
     pc_r,
     py_s,
     py_r,
+    jx_s,
+    jx_r,
     ret_s,
     ret_r,
     sq_s,
@@ -460,6 +463,9 @@
 ):
     me = lax.axis_index("ep")
     t = lax.axis_index("tp")
+    n_z = n_ep // n_x
+    slots = n_z
+    planes = slots // n_x
     z = me // n_x
     x = lax.rem(me, n_x)
     other_x = 1 - x
@@ -467,12 +473,30 @@
     across = lax.rem(t + 2, n_tp)
     diagonal = lax.rem(core + 2, n_tp)
     x_peer = z * n_x + other_x
+    block = me // slots
+    slot = lax.rem(me, slots)
+    level = slot // n_x
+    far = level + (1 - block) - 2 * level * (1 - block)
 
     def plane(offset):
         return lax.rem(z + offset, n_z)
 
     def source(offset):
         return lax.rem(z + n_z - offset, n_z)
+
+    def peer(index):
+        flip_level = 1 - index // 2
+        flip_x = lax.rem((index + 1) // 2, 2)
+        to_level = level + flip_level - 2 * level * flip_level
+        to_x = x + flip_x - 2 * x * flip_x
+        return to_level * n_x + to_x
+
+    sent = []
+
+    def go(copy):
+        copy.start()
+        sent.append(copy)
+        return copy
 
     weights = [
         pltpu.make_async_copy(w_gate.at[0], wg, w_sem.at[0]),
@@ -485,7 +509,8 @@
 
     barrier = pltpu.get_barrier_semaphore()
     greeted = [(plane(o) * n_x + x, t) for o in range(1, n_z)]
-    greeted += [(plane(o) * n_x + other_x, t) for o in range(n_z)]
+    greeted += [(block * slots + peer(i), t) for i in (1, 2)]
+    greeted += [((1 - block) * slots + peer(i), t) for i in (1, 2)]
     greeted += [(me, core), (me, across), (me, diagonal)]
     for ep, tp in greeted:
         pl.semaphore_signal(barrier, inc=1, device_id={"ep": ep, "tp": tp}, device_id_type=MESH_ID)
@@ -499,8 +524,9 @@
     normed = (x_ref[:, own_cols].astype(jnp.float32) * scale * in_gain[:, own_cols]).astype(
         jnp.bfloat16
     )
-    first_id = ids_ref[:, 0:1]
-    lane = lax.broadcasted_iota(jnp.int32, (rows, 128), 1)
+    id_rows = ids_ref[...]
+    first_id = jnp.broadcast_to(id_rows[0:1, :].astype(jnp.float32), (128, rows)).T
+    lane = lax.broadcasted_iota(jnp.int32, (rows, 128), 1).astype(jnp.float32)
     in_group = (first_id >= lane * n_x) & (first_id < lane * n_x + n_x)
     row_at = lax.broadcasted_iota(jnp.int32, (rows, rows), 0)
     col_at = lax.broadcasted_iota(jnp.int32, (rows, rows), 1)
@@ -510,186 +536,199 @@
         jnp.where(in_group, 1.0, 0.0).astype(jnp.bfloat16),
         preferred_element_type=jnp.float32,
     )
-    slot = jnp.sum(
-        jnp.where(in_group, counts + (lane * cap).astype(jnp.float32), 0.0), axis=1, keepdims=True
-    )
-    slot_at = lax.broadcasted_iota(jnp.int32, (rows, group_rows), 1).astype(jnp.float32)
-    picker[...] = jnp.where(slot_at == slot, 1.0, 0.0).astype(jnp.bfloat16)
+    place = jnp.sum(jnp.where(in_group, counts + lane * cap, 0.0), axis=1, keepdims=True)
+    place_at = lax.broadcasted_iota(jnp.int32, (rows, group_rows), 1).astype(jnp.float32)
+    picks = jnp.where(place_at == place, 1.0, 0.0)
+    picker[...] = picks.astype(jnp.bfloat16)
     x_stage[...] = lax.dot_general(
         picker[...], normed, (((0,), (0,)), ((), ())), preferred_element_type=jnp.float32
     ).astype(jnp.bfloat16)
+    odd = lax.rem(id_rows, n_x) == 1
+    mix = weight_ref[...]
+    second = jnp.sum(jnp.where(odd, mix, 0.0), axis=0, keepdims=True)
+    first = jnp.sum(jnp.where(odd, 0.0, mix), axis=0, keepdims=True)
+    at_row = lax.broadcasted_iota(jnp.int32, (8, rows), 0)
+    both = jnp.where(at_row == 0, first, jnp.where(at_row == 1, second, 0.0))
+    placed = jnp.dot(
+        both, picks, preferred_element_type=jnp.float32, precision=lax.Precision.HIGHEST
+    )
+    for g in range(n_z):
+        mix_stage[g, :, 0:cap] = placed[:, g * cap : (g + 1) * cap]
+
+    tokens = k_ref.shape[0]
+    head_dim = q_gain.shape[1]
+    heads = q_ref.shape[1] // (slots * head_dim)
+    own_tokens = tokens // n_tp
+    half_own = own_tokens // 2
+    half_tokens = tokens // 2
+    lanes = lax.broadcasted_iota(jnp.int32, (tokens, head_dim), 1)
+    low_lane = lax.rem(lanes, head_dim // 2) < head_dim // 4
+    grid_rows = tokens // GRID
+    by_row = lax.broadcasted_iota(jnp.int32, (GRID, head_dim), 1) < head_dim // 2
+
+    def table(which):
+        return jnp.concatenate(
+            [
+                jnp.where(
+                    by_row, row_table[which, pl.ds(me * grid_rows + r, 1), :], col_table[which]
+                )
+                for r in range(grid_rows)
+            ],
+            axis=0,
+        )
+
+    cosine, sine = table(0), table(1)
+    for g in range(slots):
+        cols = slice(g * head_dim, (g + 1) * head_dim)
+        k_stage[g] = turn_rows(k_ref[:, cols], k_gain[...], cosine, sine, low_lane)
+        v_stage[g] = v_ref[:, cols].T
     pl.semaphore_wait(barrier, len(greeted))
 
     def chunk_at(region, index):
         return x_all.at[region, aligned(index, cap), own_cols]
-
-    sent = []
-
-    def go(copy):
-        copy.start()
-        sent.append(copy)
-        return copy
 
     own_rows = x_stage.at[aligned(z, cap), :]
     moe_z = []
     for o in (2, 1, 3):
+        to = plane(o)
         moe_z.append(
             go(
                 remote(
-                    x_stage.at[aligned(plane(o), cap), :],
+                    x_stage.at[aligned(to, cap), :],
                     chunk_at(0, z),
                     mz_s.at[o - 1],
                     mz_r.at[o - 1],
-                    plane(o) * n_x + x,
+                    to * n_x + x,
                     t,
                 )
             )
         )
+    moe_w = []
+    for o in (2, 1, 3):
+        to = plane(o)
+        moe_w.append(
+            go(
+                remote(
+                    mix_stage.at[to], mix_all.at[z], mw_s.at[o - 1], mw_r.at[o - 1], to * n_x + x, t
+                )
+            )
+        )
     own_x = pltpu.make_async_copy(own_rows, chunk_at(0, z), own_sem.at[0])
     own_x.start()
+    own_mix = pltpu.make_async_copy(mix_stage.at[z], mix_all.at[z], own_sem.at[1])
+    own_mix.start()
+    moe_y = [[go(remote(own_rows, chunk_at(0, z), my_s.at[0, 0], my_r.at[0, 0], me, across))], []]
     moe_x = [go(remote(own_rows, chunk_at(1, z), mx_s.at[0], mx_r.at[0], x_peer, t))]
-    moe_y = [[go(remote(own_rows, chunk_at(0, z), my_s.at[0, 0], my_r.at[0, 0], me, across))], []]
-
-    tokens, kv_width = k_ref.shape
-    head_dim = q_gain.shape[1]
-    q_width = q_ref.shape[1] // n_z
-    lanes = lax.broadcasted_iota(jnp.int32, (tokens, head_dim), 1)
-    low_lane = lax.rem(lanes, head_dim // 2) < head_dim // 4
-    cosine, sine = cos_ref[...], sin_ref[...]
-    for g in range(n_z):
-        cols = slice(g * head_dim, (g + 1) * head_dim)
-        k_stage[g] = turn_rows(k_ref[:, cols], k_gain[...], cosine, sine, low_lane)
-        v_stage[g] = v_ref[:, cols].T
-
-    def k_at(region, index):
-        return k_all.at[aligned(region * n_z + index, tokens), :]
-
-    def v_at(region, index):
-        return vt_all.at[:, aligned(region * n_z + index, tokens)]
-
-    kv_z = []
-    for o in (2, 1, 3):
-        to = plane(o)
-        kv_z.append(
-            (
-                go(remote(k_stage.at[to], k_at(0, z), k_s.at[o - 1], k_r.at[o - 1], to * n_x + x, t)),
-                go(
-                    remote(
-                        v_stage.at[to], v_at(0, z), vz_s.at[o - 1], vz_r.at[o - 1], to * n_x + x, t
-                    )
-                ),
-            )
-        )
-    own_k = pltpu.make_async_copy(k_stage.at[z], k_at(0, z), own_sem.at[1])
-    own_v = pltpu.make_async_copy(v_stage.at[z], v_at(0, z), own_sem.at[2])
-    own_k.start()
-    own_v.start()
-    kv_x = [
-        go(remote(k_stage.at[z], k_at(1, z), kx_s.at[0], kx_r.at[0], x_peer, t)),
-        go(remote(v_stage.at[z], v_at(1, z), vx_s.at[0], vx_r.at[0], x_peer, t)),
-    ]
-
-    heads = q_width // head_dim
+
+    def k_at(index):
+        return k_all.at[aligned(index, tokens), :]
+
+    def v_at(index):
+        return vt_all.at[:, aligned(index, tokens)]
+
+    def near_keys(i, index):
+        to = peer(i)
+        ep = block * slots + to
+        return (
+            go(remote(k_stage.at[to], k_at(index), k_s.at[i], k_r.at[i], ep, t)),
+            go(remote(v_stage.at[to], v_at(index), v_s.at[i], v_r.at[i], ep, t)),
+        )
+
+    def near_queries(i):
+        to = peer(i)
+        ep = block * slots + to
+        go(remote(q_stage.at[to], q_all.at[slot], q_s.at[i], q_r.at[i], ep, t))
+
     to_exponent = head_dim**-0.5 * math.log2(math.e)
-    for g in range(n_z):
+    for g in range(slots):
         for h in range(heads):
             cols = slice((g * heads + h) * head_dim, (g * heads + h + 1) * head_dim)
-            q_stage[g, :, h * head_dim : (h + 1) * head_dim] = turn_rows(
-                q_ref[:, cols], q_gain[...] * to_exponent, cosine, sine, low_lane
-            )
-    for o in (1, 2, 3):
-        to = plane(o)
-        go(remote(q_stage.at[to], q_all.at[z], q_s.at[o - 1], q_r.at[o - 1], to * n_x + x, t))
-    own_q = pltpu.make_async_copy(q_stage.at[z], q_all.at[z], own_sem.at[3])
-    own_q.start()
+            turned = turn_rows(q_ref[:, cols], q_gain[...] * to_exponent, cosine, sine, low_lane)
+            for part in range(2):
+                for owner in range(n_tp):
+                    first_row = h * tokens + part * half_tokens + owner * half_own
+                    from_row = owner * own_tokens + part * half_own
+                    q_stage[g, first_row : first_row + half_own, :] = turned[
+                        from_row : from_row + half_own
+                    ]
+    own_copies = [
+        pltpu.make_async_copy(k_stage.at[slot], k_at(0), own_sem.at[2]),
+        pltpu.make_async_copy(v_stage.at[slot], v_at(0), own_sem.at[3]),
+        pltpu.make_async_copy(q_stage.at[slot], q_all.at[slot], own_sem.at[4]),
+    ]
+    for copy in own_copies:
+        copy.start()
 
     for copy, o in zip(moe_z, (2, 1, 3)):
         copy.wait_recv()
         here = chunk_at(0, source(o))
         moe_y[0].append(go(remote(here, here, my_s.at[0, o], my_r.at[0, o], me, across)))
-        moe_x.append(
-            go(remote(here, chunk_at(1, source(o)), mx_s.at[o], mx_r.at[o], x_peer, t))
-        )
+        moe_x.append(go(remote(here, chunk_at(1, source(o)), mx_s.at[o], mx_r.at[o], x_peer, t)))
     own_x.wait()
+
+    straight_keys = near_keys(0, 1)
+    near_queries(0)
+
+    def far_copies(order, cross):
+        flip = 1 - order - far + 2 * order * far
+        to_level = level + flip - 2 * level * flip
+        to = to_level * n_x + (other_x if cross else x)
+        ep = (1 - block) * slots + to
+        at = planes * (1 + 2 * cross) + far
+        send, arrive = planes * cross + order, planes * cross + far
+        return (
+            remote(k_stage.at[to], k_at(at), kf_s.at[send], kf_r.at[arrive], ep, t),
+            remote(v_stage.at[to], v_at(at), vf_s.at[send], vf_r.at[arrive], ep, t),
+        )
+
+    def send_far(cross):
+        for order in range(planes):
+            for copy in far_copies(order, cross):
+                copy.start()
+
+    def wait_far(cross):
+        for order in range(planes):
+            at, arrive = planes * (1 + 2 * cross) + order, planes * cross + order
+            remote(
+                k_stage.at[slot], k_at(at), kf_s.at[0], kf_r.at[arrive], me, core
+            ).wait_recv()
+            remote(
+                v_stage.at[slot], v_at(at), vf_s.at[0], vf_r.at[arrive], me, core
+            ).wait_recv()
+
+    send_far(0)
 
     def cols_at(region, tp):
         return x_all.at[region, :, aligned(tp, share)]
 
-    moe_c = [[], []]
-    moe_c[0].append(
-        go(remote(cols_at(0, t), cols_at(0, t), mc_s.at[0, 0], mc_r.at[0, 0], me, core))
-    )
+    def to_core(region, index, tp):
+        return go(
+            remote(
+                cols_at(region, tp),
+                cols_at(region, tp),
+                mc_s.at[region, index],
+                mc_r.at[region, index],
+                me,
+                core,
+            )
+        )
+
+    moe_c = [[to_core(0, 0, t)], []]
     for copy, o in zip(moe_x, (0, 2, 1, 3)):
         copy.wait_recv()
         here = chunk_at(1, source(o))
         moe_y[1].append(go(remote(here, here, my_s.at[1, o], my_r.at[1, o], me, across)))
-    moe_c[1].append(
-        go(remote(cols_at(1, t), cols_at(1, t), mc_s.at[1, 0], mc_r.at[1, 0], me, core))
-    )
+    moe_c[1].append(to_core(1, 0, t))
+    near_queries(2)
+    near_queries(1)
+    crossed_keys = near_keys(2, slots) + near_keys(1, slots + 1)
+    send_far(1)
     for copy in moe_y[0]:
         copy.wait_recv()
-    moe_c[0].append(
-        go(remote(cols_at(0, across), cols_at(0, across), mc_s.at[0, 1], mc_r.at[0, 1], me, core))
-    )
-
-    def forward_keys(index, o):
-        key_copy, value_copy = kv_z[index]
-        key_copy.wait_recv()
-        kv_x.append(
-            go(
-                remote(
-                    k_at(0, source(o)), k_at(1, source(o)), kx_s.at[o], kx_r.at[o], x_peer, t
-                )
-            )
-        )
-        value_copy.wait_recv()
-        kv_x.append(
-            go(
-                remote(
-                    v_at(0, source(o)), v_at(1, source(o)), vx_s.at[o], vx_r.at[o], x_peer, t
-                )
-            )
-        )
+    moe_c[0].append(to_core(0, 1, across))
 
     blocks = (core, diagonal, t, across)
     inner_width = wg.shape[1]
-
-    def experts(region):
-        for copy in moe_c[region]:
-            copy.wait_recv()
-        if region == 0:
-            weights[0].wait()
-            weights[1].wait()
-
-        def pre(index, carry):
-            cols = aligned(index, FF_STEP)
-            rows_in = x_all[region]
-            gate = jnp.dot(rows_in, wg[:, cols], preferred_element_type=jnp.float32)
-            up = jnp.dot(rows_in, wu[:, cols], preferred_element_type=jnp.float32)
-            hidden[:, cols] = (gate / (1.0 + jnp.exp(-gate)) * up).astype(jnp.bfloat16)
-            return carry
-
-        lax.fori_loop(0, inner_width // FF_STEP, pre, 0)
-        if region == 0:
-            weights[2].wait()
-        for index, block in enumerate(blocks):
-            part = jnp.dot(
-                hidden[...], wd[:, aligned(block, share)], preferred_element_type=jnp.float32
-            ).astype(jnp.bfloat16)
-            if index < 2:
-                part_send[region, index] = part
-                go(
-                    remote(
-                        part_send.at[region, index],
-                        part_recv.at[region, index],
-                        pc_s.at[region, index],
-                        pc_r.at[region, index],
-                        me,
-                        core,
-                    )
-                )
-            else:
-                part_keep[region, index - 2] = part
 
     def part_copy(region, index):
         return remote(
@@ -701,6 +740,36 @@
             core,
         )
 
+    def experts(region):
+        for copy in moe_c[region]:
+            copy.wait_recv()
+        if region == 0:
+            weights[0].wait()
+            weights[1].wait()
+
+        def pre(index, carry):
+            cols = aligned(index, FF_STEP)
+            rows_now = x_all[region]
+            gate = jnp.dot(rows_now, wg[:, cols], preferred_element_type=jnp.float32)
+            up = jnp.dot(rows_now, wu[:, cols], preferred_element_type=jnp.float32)
+            hidden[:, cols] = (gate / (1.0 + jnp.exp(-gate)) * up).astype(jnp.bfloat16)
+            return carry
+
+        lax.fori_loop(0, inner_width // FF_STEP, pre, 0)
+        if region == 0:
+            weights[2].wait()
+        for index in (1, 0, 3, 2):
+            part = jnp.dot(
+                hidden[...],
+                wd[:, aligned(blocks[index], share)],
+                preferred_element_type=jnp.float32,
+            ).astype(jnp.bfloat16)
+            if index < 2:
+                part_send[region, index] = part
+                go(part_copy(region, index))
+            else:
+                part_keep[region, index - 2] = part
+
     def pair_copy(region):
         return remote(
             pair_send.at[region], pair_recv.at[region], py_s.at[region], py_r.at[region], me, across
@@ -711,42 +780,63 @@
         pair_send[region] = (
             part_keep[region, 1].astype(jnp.float32) + part_recv[region, 1].astype(jnp.float32)
         ).astype(jnp.bfloat16)
-        sent.append(pair_copy(region))
-        sent[-1].start()
+        pair_copy(region).start()
 
     experts(0)
-    pair(0)
-    forward_keys(0, 2)
-    forward_keys(1, 1)
+    step = 2 * tokens
+    queries = heads * tokens
+
+    def key_step(index):
+        return slice(index * step, (index + 1) * step)
+
+    def load_state(to):
+        return tops[to, 0:1, :], totals[to, 0:1, :], accs[to]
+
+    def save_state(to, state):
+        tops[to, 0:1, :], totals[to, 0:1, :], accs[to] = state
+
+    def own_block(turn, carry):
+        index = lax.rem(turn + slots - 1, slots)
+        to = peer(index)
+
+        @pl.when(index < slots - 1)
+        def _():
+            remote(
+                q_stage.at[to], q_all.at[to], q_s.at[index], q_r.at[index], me, core
+            ).wait_recv()
+
+        state = (
+            jnp.full((1, queries), -1e30, jnp.float32),
+            jnp.zeros((1, queries), jnp.float32),
+            jnp.zeros((head_dim, queries), jnp.float32),
+        )
+        for s in range(slots // 2):
+            state = attend_keys(q_all[to], k_all[key_step(s), :], vt_all[:, key_step(s)], state)
+        save_state(to, state)
+
+        @pl.when(turn == 0)
+        def _():
+            pair(1)
+
+        return carry
+
     for copy in moe_y[1]:
         copy.wait_recv()
-    moe_c[1].append(
-        go(remote(cols_at(1, across), cols_at(1, across), mc_s.at[1, 1], mc_r.at[1, 1], me, core))
-    )
-    forward_keys(2, 3)
+    moe_c[1].append(to_core(1, 1, across))
+    pair(0)
     experts(1)
-    pair(1)
-
-    def return_copy(region, o):
-        to = plane(o)
-        return remote(
-            rows_out.at[region, aligned(to, cap), :],
-            returned.at[aligned(x * n_z + z, cap), :],
-            ret_s.at[region, o],
-            ret_r.at[region, o],
-            to * n_x + (x if region == 0 else other_x),
-            t,
-        )
-
-    own_return = pltpu.make_async_copy(
-        rows_out.at[0, aligned(z, cap), :],
-        returned.at[aligned(x * n_z + z, cap), :],
-        own_sem.at[4],
-    )
-    returns = [(0, o) for o in range(1, n_z)] + [(1, o) for o in range(n_z)]
-
-    def send_back():
-        for region in range(n_x):
+    for copy in own_copies:
+        copy.wait()
+    for copy in straight_keys:
+        copy.wait_recv()
+    wait_far(0)
+    lax.fori_loop(0, slots, own_block, 0)
+
+    join = remote(rows_out.at[1], rows_in, jx_s.at[0], jx_r.at[0], x_peer, t)
+    sent.append(join)
+
+    def expert_rows():
+        for region in (1, 0):
             part_copy(region, 0).wait_recv()
             pair_copy(region).wait_recv()
             rows_out[region] = (
@@ -754,116 +844,196 @@
                 + part_recv[region, 0].astype(jnp.float32)
                 + pair_recv[region].astype(jnp.float32)
             ).astype(jnp.bfloat16)
-        for region, o in returns:
-            return_copy(region, o).start()
-        own_return.start()
-
-    for copy in kv_x:
+            if region == 1:
+                join.start()
+
+    for copy in crossed_keys:
         copy.wait_recv()
-    own_k.wait()
-    own_v.wait()
-    own_q.wait()
-
-    def output_copy(o):
+
+    def near_block(index, carry):
+        to = peer(index)
+        s = slots // 2
+        save_state(
+            to,
+            attend_keys(q_all[to], k_all[key_step(s), :], vt_all[:, key_step(s)], load_state(to)),
+        )
+        @pl.when(index == 1)
+        def _():
+            expert_rows()
+
+        return carry
+
+    lax.fori_loop(0, slots, near_block, 0)
+
+    def output_copy(index, part):
+        to = peer(index)
+        at = slice(part * half_tokens, (part + 1) * half_tokens)
+        return remote(
+            o_stage.at[to, :, at, :],
+            o_all.at[pl.ds(slot * heads, heads), at, :],
+            o_s.at[part, index],
+            o_r.at[part, index],
+            block * slots + to,
+            t,
+        )
+
+    def last_block(index, carry):
+        to = peer(index)
+        s = slots // 2 + 1
+        _, total, acc = attend_keys(
+            q_all[to], k_all[key_step(s), :], vt_all[:, key_step(s)], load_state(to)
+        )
+        out = (acc / total).T.astype(jnp.bfloat16)
+        for h in range(heads):
+            o_stage[to, h] = out[h * tokens : (h + 1) * tokens]
+
+        @pl.when(index == 0)
+        def _():
+            output_copy(0, 0).start()
+
+        @pl.when(index == 1)
+        def _():
+            output_copy(1, 0).start()
+            output_copy(0, 1).start()
+            output_copy(1, 1).start()
+
+        @pl.when(index == 2)
+        def _():
+            output_copy(2, 0).start()
+            output_copy(2, 1).start()
+
+        return carry
+
+    wait_far(1)
+    lax.fori_loop(0, slots, last_block, 0)
+    own_o = pltpu.make_async_copy(
+        o_stage.at[slot], o_all.at[pl.ds(slot * heads, heads)], own_sem.at[6]
+    )
+    own_o.start()
+
+    weights[3].wait()
+    own_o.wait()
+
+    out_width = wo.shape[1]
+    all_heads = slots * heads
+
+    pieces = 2
+    piece_width = out_width // pieces
+
+    def project(part):
+        at = slice(part * half_tokens, (part + 1) * half_tokens)
+        taken = jnp.concatenate([o_all[h, at, :] for h in range(all_heads)], axis=1)
+        copies = []
+        for piece in range(pieces):
+
+            def columns(index, carry):
+                cols = aligned(index, 512)
+                out = jnp.dot(taken, wo[:, cols], preferred_element_type=jnp.float32).astype(
+                    jnp.bfloat16
+                )
+                for owner in range(n_tp):
+                    head_part[part, owner, :, cols] = out[owner * half_own : (owner + 1) * half_own]
+                return carry
+
+            lax.fori_loop(
+                piece * piece_width // 512, (piece + 1) * piece_width // 512, columns, 0
+            )
+            cols = slice(piece * piece_width, (piece + 1) * piece_width)
+            copies.append(
+                [
+                    go(
+                        remote(
+                            head_part.at[part, to, :, cols],
+                            head_recv.at[part, i, :, cols],
+                            hc_s.at[part, piece, i],
+                            hc_r.at[part, piece, i],
+                            me,
+                            core,
+                        )
+                    )
+                    for i, to in ((1, diagonal), (0, core))
+                ]
+            )
+        return copies
+
+    def to_across(part, copies):
+        sums = []
+        for piece in range(pieces):
+            cols = slice(piece * piece_width, (piece + 1) * piece_width)
+            copies[piece][0].wait_recv()
+            head_pair[part, :, cols] = (
+                head_part[part, across, :, cols].astype(jnp.float32)
+                + head_recv[part, 1, :, cols].astype(jnp.float32)
+            ).astype(jnp.bfloat16)
+            sums.append(
+                go(
+                    remote(
+                        head_pair.at[part, :, cols],
+                        head_last.at[part, :, cols],
+                        hy_s.at[part, piece],
+                        hy_r.at[part, piece],
+                        me,
+                        across,
+                    )
+                )
+            )
+        return sums
+
+    for i in (0, 1, 2):
+        output_copy(i, 0).wait_recv()
+    first_half = project(0)
+    first_y = to_across(0, first_half)
+    for copy in moe_w:
+        copy.wait_recv()
+    own_mix.wait()
+    join.wait_recv()
+    mine_first = x == 0
+    for g in range(n_z):
+        mix_cols = mix_all[g].T
+        here = slice(g * cap, (g + 1) * cap)
+        mine = rows_out[0, here, :].astype(jnp.float32)
+        theirs = rows_in[here, :].astype(jnp.float32)
+        first_w, second_w = mix_cols[0:cap, 0:1], mix_cols[0:cap, 1:2]
+        joined[here, :] = (
+            mine * jnp.where(mine_first, first_w, second_w)
+            + theirs * jnp.where(mine_first, second_w, first_w)
+        ).astype(jnp.bfloat16)
+
+    def back_at():
+        return returned.at[aligned(z, cap), :]
+
+    own_return = pltpu.make_async_copy(joined.at[aligned(z, cap), :], back_at(), own_sem.at[5])
+    own_return.start()
+    returns = []
+    for o in (2, 1, 3):
         to = plane(o)
-        return remote(
-            o_stage.at[to],
-            o_all.at[:, aligned(z, q_width)],
-            o_s.at[o - 1],
-            o_r.at[o - 1],
-            to * n_x + x,
-            t,
-        )
-
-    def block(index, carry):
-        o = index + 1
-        to = plane(o)
-
-        @pl.when(o < n_z)
-        def _():
-            back = n_z - o
-            remote(
-                q_stage.at[to], q_all.at[to], q_s.at[back - 1], q_r.at[back - 1], me, core
-            ).wait_recv()
-
-        for h in range(heads):
-            cols = slice(h * head_dim, (h + 1) * head_dim)
-            o_stage[to, :, cols] = attend_heads(q_all[to, :, cols], k_all, vt_all, None)
-
-        @pl.when(o < n_z)
-        def _():
-            output_copy(o).start()
-
-        @pl.when(o == n_z // 2)
-        def _():
-            send_back()
-
-        return carry
-
-    lax.fori_loop(0, n_z, block, 0)
-    own_o = pltpu.make_async_copy(
-        o_stage.at[z], o_all.at[:, aligned(z, q_width)], own_sem.at[5]
-    )
-    own_o.start()
-    weights[3].wait()
-    for o in range(1, n_z):
-        output_copy(o).wait_recv()
-    own_o.wait()
-
-    own_tokens = tokens // n_tp
-    out_width = wo.shape[1]
-
-    def project(first, second, into):
-        taken = jnp.concatenate(
-            [o_all[aligned(first, own_tokens), :], o_all[aligned(second, own_tokens), :]], axis=0
-        )
-
-        def columns(index, carry):
-            cols = aligned(index, 512)
-            part = jnp.dot(taken, wo[:, cols], preferred_element_type=jnp.float32).astype(
-                jnp.bfloat16
+        returns.append(
+            go(
+                remote(
+                    joined.at[aligned(to, cap), :],
+                    back_at(),
+                    ret_s.at[o - 1],
+                    ret_r.at[o - 1],
+                    to * n_x + x,
+                    t,
+                )
             )
-            into[0, :, cols] = part[:own_tokens]
-            into[1, :, cols] = part[own_tokens:]
-            return carry
-
-        lax.fori_loop(0, out_width // 512, columns, 0)
-
-    project(core, diagonal, head_send)
-    head_c = [
-        go(remote(head_send.at[i], head_recv.at[i], hc_s.at[i], hc_r.at[i], me, core))
-        for i in (1, 0)
-    ]
-    project(t, across, head_keep)
-    head_c[0].wait_recv()
-    head_pair[...] = (
-        head_keep[1].astype(jnp.float32) + head_recv[1].astype(jnp.float32)
-    ).astype(jnp.bfloat16)
-    head_y = go(remote(head_pair, head_last, hy_s.at[0], hy_r.at[0], me, across))
-
-    for region, o in returns:
-        return_copy(region, o).wait_recv()
+        )
+    for i in (0, 1, 2):
+        output_copy(i, 1).wait_recv()
+    second_half = project(1)
+    second_y = to_across(1, second_half)
+    for copy in returns:
+        copy.wait_recv()
     own_return.wait()
-    picks = picker[...]
-    ids = ids_ref[...]
-    mix = weight_ref[...]
-    combined = jnp.zeros((rows, share), jnp.float32)
-    for parity in range(n_x):
-        gathered = jnp.dot(
-            picks,
-            returned[parity * group_rows : (parity + 1) * group_rows, :],
-            preferred_element_type=jnp.float32,
-        )
-        factor = jnp.sum(
-            jnp.where(lax.rem(ids, n_x) == parity, mix, 0.0), axis=1, keepdims=True
-        )
-        combined = combined + gathered * factor
+    combined = jnp.dot(picker[...], returned[...], preferred_element_type=jnp.float32)
     squares = jnp.sum(combined * combined, axis=1, keepdims=True)
     squares_send[...] = jnp.broadcast_to(squares, (rows, 128)).T[0:8, :]
     square_copies = [
         go(remote(squares_send, squares_recv.at[i], sq_s.at[i], sq_r.at[i], me, tp))
         for i, tp in enumerate((core, across, diagonal))
     ]
+
     for copy in square_copies:
         copy.wait_recv()
     all_squares = squares_send[...] + squares_recv[0] + squares_recv[1] + squares_recv[2]
@@ -872,38 +1042,48 @@
         jnp.bfloat16
     )
 
-    head_c[1].wait_recv()
-    head_y.wait_recv()
-    mixed = (
-        head_keep[0].astype(jnp.float32)
-        + head_recv[0].astype(jnp.float32)
-        + head_last[...].astype(jnp.float32)
-    )
-    mean = jnp.mean(mixed * mixed, axis=1, keepdims=True)
-    mixer_out[...] = (mixed * lax.rsqrt(mean + EPS) * mixer_gain[...]).astype(jnp.bfloat16)
+    for part, copies, last in ((0, first_half, first_y), (1, second_half, second_y)):
+        for piece in range(pieces):
+            copies[piece][1].wait_recv()
+            last[piece].wait_recv()
+        mixed = (
+            head_part[part, t].astype(jnp.float32)
+            + head_recv[part, 0].astype(jnp.float32)
+            + head_last[part].astype(jnp.float32)
+        )
+        mean = jnp.mean(mixed * mixed, axis=1, keepdims=True)
+        mixer_out[part * half_own : (part + 1) * half_own, :] = (
+            mixed * lax.rsqrt(mean + EPS) * mixer_gain[...]
+        ).astype(jnp.bfloat16)
 
     for copy in sent:
         copy.wait_send()
-    for o in range(1, n_z):
-        output_copy(o).wait_send()
-    for region, o in returns:
-        return_copy(region, o).wait_send()
-
-
-def turn_tables(row_count, row_offset, head_dim):
-    position = row_offset + jnp.arange(row_count, dtype=jnp.int32)
+    for region in range(n_x):
+        pair_copy(region).wait_send()
+    for cross in range(n_x):
+        for order in range(planes):
+            for copy in far_copies(order, cross):
+                copy.wait_send()
+    for i in (0, 1, 2):
+        for part in range(2):
+            output_copy(i, part).wait_send()
+
+
+def turn_tables(row_count, head_dim):
     half_width = head_dim // 2
-    frequency = THETA ** (-jnp.arange(0, half_width, 2, dtype=jnp.float32) / half_width)
-    row_angle = (position // GRID).astype(jnp.float32)[:, None] * frequency[None, :]
-    col_angle = (position % GRID).astype(jnp.float32)[:, None] * frequency[None, :]
-    angles = jnp.concatenate([row_angle, row_angle, col_angle, col_angle], axis=1)
-    lane = jnp.arange(head_dim, dtype=jnp.int32)[None, :]
-    sign = jnp.where(lane % half_width < half_width // 2, -1.0, 1.0)
-    return jnp.cos(angles), jnp.sin(angles) * sign
+    steps = np.arange(0, half_width, 2, dtype=np.float32) / np.float32(half_width)
+    frequency = np.float32(THETA) ** -steps
+    sign = np.where(np.arange(half_width) < half_width // 2, -1.0, 1.0)
+    tables = []
+    for count in (row_count, GRID):
+        angles = np.arange(count, dtype=np.float32)[:, None] * frequency[None, :]
+        angles = np.tile(angles, (1, 2)).astype(np.float64)
+        both = np.stack([np.cos(angles), np.sin(angles) * sign])
+        tables.append(np.tile(both, (1, 1, 2)).astype(np.float32))
+    return tables
 
 
 def layer(
-    n_z,
     n_x,
     query_rows,
     key_rows,
@@ -921,38 +1101,48 @@
     w_down,
     out_gain,
 ):
+    n_ep = lax.axis_size("ep")
     n_tp = lax.axis_size("tp")
+    n_z = n_ep // n_x
+    slots = n_z
     tokens = query_rows.shape[0]
     head_dim = query_gain.shape[0]
+    heads = query_rows.shape[1] // (slots * head_dim)
     rows, width = expert_input.shape
     share = width // n_tp
     inner = w_gate.shape[2]
-    q_width = query_rows.shape[1] // n_z
     cap = -(-(3 * rows // (4 * n_x)) // 16) * 16
-    cosine, sine = turn_tables(tokens, lax.axis_index("ep") * tokens, head_dim)
+    row_table, col_table = turn_tables(n_ep * tokens // GRID, head_dim)
     bf16, f32 = jnp.bfloat16, jnp.float32
     vmem = pl.BlockSpec(memory_space=pltpu.VMEM)
     hbm = pl.BlockSpec(memory_space=pl.ANY)
     dma = pltpu.SemaphoreType.DMA
     group_rows = n_z * cap
     own_tokens = tokens // n_tp
-    far = n_z - 1
+    half_own = own_tokens // 2
+    queries = heads * tokens
+    keys = n_ep * tokens
     scratch = [
         pltpu.VMEM(w_gate.shape[1:], bf16),
         pltpu.VMEM(w_up.shape[1:], bf16),
         pltpu.VMEM(w_down.shape[1:], bf16),
         pltpu.VMEM(w_out.shape, bf16),
-        pltpu.VMEM((n_z, tokens, q_width), bf16),
-        pltpu.VMEM((n_z, tokens, head_dim), bf16),
-        pltpu.VMEM((n_z, head_dim, tokens), bf16),
-        pltpu.VMEM((n_x * n_z * tokens, head_dim), bf16),
-        pltpu.VMEM((head_dim, n_x * n_z * tokens), bf16),
-        pltpu.VMEM((n_z, tokens, q_width), bf16),
-        pltpu.VMEM((n_z, tokens, q_width), bf16),
-        pltpu.VMEM((tokens, n_z * q_width), bf16),
+        pltpu.VMEM((slots, queries, head_dim), bf16),
+        pltpu.VMEM((slots, tokens, head_dim), bf16),
+        pltpu.VMEM((slots, head_dim, tokens), bf16),
+        pltpu.VMEM((keys, head_dim), bf16),
+        pltpu.VMEM((head_dim, keys), bf16),
+        pltpu.VMEM((slots, queries, head_dim), bf16),
+        pltpu.VMEM((slots, 8, queries), f32),
+        pltpu.VMEM((slots, 8, queries), f32),
+        pltpu.VMEM((slots, head_dim, queries), f32),
+        pltpu.VMEM((slots, heads, tokens, head_dim), bf16),
+        pltpu.VMEM((slots * heads, tokens, head_dim), bf16),
         pltpu.VMEM((rows, group_rows), bf16),
         pltpu.VMEM((group_rows, share), bf16),
         pltpu.VMEM((n_x, group_rows, width), bf16),
+        pltpu.VMEM((n_z, 8, 128), f32),
+        pltpu.VMEM((n_z, 8, 128), f32),
         pltpu.VMEM((group_rows, inner), bf16),
         pltpu.VMEM((n_x, 2, group_rows, share), bf16),
         pltpu.VMEM((n_x, 2, group_rows, share), bf16),
@@ -960,38 +1150,41 @@
         pltpu.VMEM((n_x, group_rows, share), bf16),
         pltpu.VMEM((n_x, group_rows, share), bf16),
         pltpu.VMEM((n_x, group_rows, share), bf16),
-        pltpu.VMEM((n_x * group_rows, share), bf16),
+        pltpu.VMEM((group_rows, share), bf16),
+        pltpu.VMEM((group_rows, share), bf16),
+        pltpu.VMEM((group_rows, share), bf16),
         pltpu.VMEM((8, rows), f32),
         pltpu.VMEM((3, 8, rows), f32),
-        pltpu.VMEM((2, own_tokens, width), bf16),
-        pltpu.VMEM((2, own_tokens, width), bf16),
-        pltpu.VMEM((2, own_tokens, width), bf16),
-        pltpu.VMEM((own_tokens, width), bf16),
-        pltpu.VMEM((own_tokens, width), bf16),
+        pltpu.VMEM((2, n_tp, half_own, width), bf16),
+        pltpu.VMEM((2, 2, half_own, width), bf16),
+        pltpu.VMEM((2, half_own, width), bf16),
+        pltpu.VMEM((2, half_own, width), bf16),
         dma((4,)),
-        dma((6,)),
+        dma((7,)),
     ]
     for shape in (
-        (far,),
+        (n_z - 1,),
+        (n_z - 1,),
         (n_z,),
         (n_x, n_z),
         (n_x, 2),
-        (far,),
-        (far,),
-        (n_z,),
-        (n_z,),
-        (far,),
-        (far,),
+        (slots - 1,),
+        (slots - 1,),
+        (slots,),
+        (slots,),
+        (slots - 1,),
+        (2, slots - 1),
         (n_x, 2),
         (n_x,),
-        (n_x, n_z),
+        (1,),
+        (n_z - 1,),
         (3,),
-        (2,),
-        (1,),
+        (2, 2, 2),
+        (2, 2),
     ):
         scratch += [dma(shape), dma(shape)]
     return pl.pallas_call(
-        functools.partial(layer_kernel, n_z, n_x, n_tp, cap),
+        functools.partial(layer_kernel, n_ep, n_x, n_tp, cap),
         in_specs=[vmem] * 13 + [hbm] * 4,
         out_specs=(vmem, vmem),
         out_shape=(
@@ -1007,14 +1200,14 @@
         query_rows,
         key_rows,
         value_rows,
-        cosine,
-        sine,
+        jnp.asarray(row_table),
+        jnp.asarray(col_table),
         query_gain[None, :],
         key_gain[None, :],
         mixer_gain[None, :],
         expert_input,
-        expert_ids,
-        expert_weights,
+        expert_ids.T,
+        expert_weights.T,
         input_gain[None, :],
         out_gain[None, :],
         w_gate,
@@ -1042,18 +1235,18 @@
     out_gain,
 ):
     n_ep = lax.axis_size("ep")
-    n_z = key_rows.shape[1] // query_gain.shape[0]
     n_x = w_gate.shape[0] * n_ep // GROUPS
+    kv_heads = key_rows.shape[1] // query_gain.shape[0]
     if (
-        n_z == GROUPS
-        and n_z * n_x == n_ep
+        kv_heads == GROUPS
+        and GROUPS * n_x == n_ep
         and n_x == 2
         and expert_ids.shape[1] == n_x
         and w_gate.shape[0] == 1
         and lax.axis_size("tp") == 4
+        and query_rows.shape[0] % GRID == 0
     ):
         return layer(
-            n_z,
             n_x,
             query_rows,
             key_rows,

time: 108 us -> 87.1 us (0.81)
  the two profiles are of different devices: /device:TPU:9 before, /device:TPU:0 now
where the time goes in v2:
time: 87.1 us; the launch traced here: 86.9 us
  Pallas kernels  82.9 us (95%)
  local copies, waits for them, and re-layouts  3.38 us (4%)
    pallas_call x1, Pallas kernels, layer(): pl.pallas_call(functools.partial(layer_kernel, n_ep, n_x, n_tp, cap), in_...  82.9 us
    unnamed x2, local copies, waits for them, and re-layouts  3.38 us

profile of v2, /device:TPU:0, one launch (start us, length us, event | category | flops | bytes accessed | tf_op | source)
XLA Modules:
  0.0 86.9 jit_solution(8330370953716239910)
XLA Ops:
  0.6 82.9 %layer.1 = (bf16[96,2048]{1,0:T(8,128)(2,1)}, bf16[192,512]{1,0:T(8,128)(2,1)}) custom-call(bf16[384,1024]{1,0:T(8,128)(2,1)} %q_ref.1, bf16[384,512]{1,0:T(8,128)(2,1)} %k_ref.1, bf16[384,512]{1,0:T(8,128)(2,1)} %v_ref.1, f32[2,48,128]{2,1,0:T(8,128)} %constant.4.clone.row_table, f32[2,64,128]{2,1,0:T(8,128)} %constant.5.clone.col_table, ...), custom_call_target="tpu_custom_call" | custom-call | tf_op jit(solution)/shard_map/layer/pallas_call | solution.py:1186
  83.5 1.8 %copy.21 = bf16[96,2048]{1,0:T(8,128)(2,1)} copy(bf16[96,2048]{1,0:T(8,128)(2,1)} %get-tuple-element.4) | data formatting | bytes 786432
  85.3 1.6 %copy.22 = bf16[192,512]{1,0:T(8,128)(2,1)} copy(bf16[192,512]{1,0:T(8,128)(2,1)} %get-tuple-element.5) | data formatting | bytes 393216

commit v3 on v2

--- a/solution.py
+++ b/solution.py
@@ -362,11 +362,21 @@
     return new_top, total, acc
 
 
+def load_inputs(n_ep, n_x, n_tp, cap, count, *refs):
+    held, weights, outs = refs[:count], refs[count : count + 4], refs[count + 4 : count + 6]
+    loaded, sems, rest = refs[count + 6 : 2 * count + 6], refs[2 * count + 6], refs[2 * count + 7 :]
+    loads = [pltpu.make_async_copy(held[i], loaded[i], sems.at[i]) for i in range(count)]
+    for i in (8, 9, 10, 11, 1, 6, 3, 4, 2, 0, 5, 7, 12):
+        loads[i].start()
+    layer_kernel(n_ep, n_x, n_tp, cap, loads, *loaded, *weights, *outs, *rest)
+
+
 def layer_kernel(
     n_ep,
     n_x,
     n_tp,
     cap,
+    loads,
     q_ref,
     k_ref,
     v_ref,
@@ -485,7 +495,7 @@
         return lax.rem(z + n_z - offset, n_z)
 
     def peer(index):
-        flip_level = 1 - index // 2
+        flip_level = lax.rem(index + 1, 2) * (1 - index // 3)
         flip_x = lax.rem((index + 1) // 2, 2)
         to_level = level + flip_level - 2 * level * flip_level
         to_x = x + flip_x - 2 * x * flip_x
@@ -504,8 +514,6 @@
         pltpu.make_async_copy(w_down.at[0], wd, w_sem.at[2]),
         pltpu.make_async_copy(w_out, wo, w_sem.at[3]),
     ]
-    for copy in weights:
-        copy.start()
 
     barrier = pltpu.get_barrier_semaphore()
     greeted = [(plane(o) * n_x + x, t) for o in range(1, n_z)]
@@ -514,6 +522,12 @@
     greeted += [(me, core), (me, across), (me, diagonal)]
     for ep, tp in greeted:
         pl.semaphore_signal(barrier, inc=1, device_id={"ep": ep, "tp": tp}, device_id_type=MESH_ID)
+
+    for i in (8, 9, 10, 11):
+        loads[i].wait()
+
+    for copy in weights:
+        copy.start()
 
     rows, width = x_ref.shape
     share = width // n_tp
@@ -555,6 +569,8 @@
     for g in range(n_z):
         mix_stage[g, :, 0:cap] = placed[:, g * cap : (g + 1) * cap]
 
+    for i in (1, 2, 3, 4, 6):
+        loads[i].wait()
     tokens = k_ref.shape[0]
     head_dim = q_gain.shape[1]
     heads = q_ref.shape[1] // (slots * head_dim)
@@ -639,6 +655,10 @@
         ep = block * slots + to
         go(remote(q_stage.at[to], q_all.at[slot], q_s.at[i], q_r.at[i], ep, t))
 
+    straight_keys = near_keys(0, 1)
+
+    for i in (0, 5, 7, 12):
+        loads[i].wait()
     to_exponent = head_dim**-0.5 * math.log2(math.e)
     for g in range(slots):
         for h in range(heads):
@@ -666,7 +686,6 @@
         moe_x.append(go(remote(here, chunk_at(1, source(o)), mx_s.at[o], mx_r.at[o], x_peer, t)))
     own_x.wait()
 
-    straight_keys = near_keys(0, 1)
     near_queries(0)
 
     def far_copies(order, cross):
@@ -686,8 +705,8 @@
             for copy in far_copies(order, cross):
                 copy.start()
 
-    def wait_far(cross):
-        for order in range(planes):
+    def wait_far(cross, orders):
+        for order in orders:
             at, arrive = planes * (1 + 2 * cross) + order, planes * cross + order
             remote(
                 k_stage.at[slot], k_at(at), kf_s.at[0], kf_r.at[arrive], me, core
@@ -697,6 +716,8 @@
             ).wait_recv()
 
     send_far(0)
+    near_queries(1)
+    near_queries(2)
 
     def cols_at(region, tp):
         return x_all.at[region, :, aligned(tp, share)]
@@ -719,9 +740,7 @@
         here = chunk_at(1, source(o))
         moe_y[1].append(go(remote(here, here, my_s.at[1, o], my_r.at[1, o], me, across)))
     moe_c[1].append(to_core(1, 0, t))
-    near_queries(2)
-    near_queries(1)
-    crossed_keys = near_keys(2, slots) + near_keys(1, slots + 1)
+    crossed_keys = near_keys(1, slots) + near_keys(2, slots + 1)
     send_far(1)
     for copy in moe_y[0]:
         copy.wait_recv()
@@ -829,7 +848,7 @@
         copy.wait()
     for copy in straight_keys:
         copy.wait_recv()
-    wait_far(0)
+    wait_far(0, range(planes))
     lax.fori_loop(0, slots, own_block, 0)
 
     join = remote(rows_out.at[1], rows_in, jx_s.at[0], jx_r.at[0], x_peer, t)
@@ -857,7 +876,7 @@
             to,
             attend_keys(q_all[to], k_all[key_step(s), :], vt_all[:, key_step(s)], load_state(to)),
         )
-        @pl.when(index == 1)
+        @pl.when(index == 0)
         def _():
             expert_rows()
 
@@ -877,34 +896,46 @@
             t,
         )
 
-    def last_block(index, carry):
+    def last_block(turn, carry):
+        index = lax.rem(2 * slots - 2 - turn, slots)
         to = peer(index)
-        s = slots // 2 + 1
+        at = keys_of(2 * slots - 1)
         _, total, acc = attend_keys(
-            q_all[to], k_all[key_step(s), :], vt_all[:, key_step(s)], load_state(to)
+            q_all[to], k_all[at, :], vt_all[:, at], load_state(to)
         )
         out = (acc / total).T.astype(jnp.bfloat16)
         for h in range(heads):
             o_stage[to, h] = out[h * tokens : (h + 1) * tokens]
 
-        @pl.when(index == 0)
+        @pl.when(turn == 0)
+        def _():
+            output_copy(2, 0).start()
+
+        @pl.when(turn == 1)
+        def _():
+            output_copy(1, 0).start()
+
+        @pl.when(turn == 2)
         def _():
             output_copy(0, 0).start()
-
-        @pl.when(index == 1)
-        def _():
-            output_copy(1, 0).start()
-            output_copy(0, 1).start()
-            output_copy(1, 1).start()
-
-        @pl.when(index == 2)
-        def _():
-            output_copy(2, 0).start()
-            output_copy(2, 1).start()
+            for i in (2, 0, 1):
+                output_copy(i, 1).start()
 
         return carry
 
-    wait_far(1)
+    wait_far(1, (0,))
+
+    def keys_of(index):
+        return slice(index * tokens, (index + 1) * tokens)
+
+    def next_block(index, carry):
+        to = peer(index)
+        at = keys_of(2 * slots - 2)
+        save_state(to, attend_keys(q_all[to], k_all[at, :], vt_all[:, at], load_state(to)))
+        return carry
+
+    lax.fori_loop(0, slots, next_block, 0)
+    wait_far(1, (1,))
     lax.fori_loop(0, slots, last_block, 0)
     own_o = pltpu.make_async_copy(
         o_stage.at[slot], o_all.at[pl.ds(slot * heads, heads)], own_sem.at[6]
@@ -1067,6 +1098,11 @@
     for i in (0, 1, 2):
         for part in range(2):
             output_copy(i, part).wait_send()
+
+
+def hand_over(mixer_in, moe_in, mixer_out, moe_out):
+    mixer_out[...] = mixer_in[...]
+    moe_out[...] = moe_in[...]
 
 
 def turn_tables(row_count, head_dim):
@@ -1115,14 +1151,31 @@
     row_table, col_table = turn_tables(n_ep * tokens // GRID, head_dim)
     bf16, f32 = jnp.bfloat16, jnp.float32
     vmem = pl.BlockSpec(memory_space=pltpu.VMEM)
-    hbm = pl.BlockSpec(memory_space=pl.ANY)
+    hbm = pl.BlockSpec(memory_space=pltpu.HBM)
     dma = pltpu.SemaphoreType.DMA
     group_rows = n_z * cap
     own_tokens = tokens // n_tp
     half_own = own_tokens // 2
     queries = heads * tokens
     keys = n_ep * tokens
-    scratch = [
+    inputs = (
+        query_rows,
+        key_rows,
+        value_rows,
+        jnp.asarray(row_table),
+        jnp.asarray(col_table),
+        query_gain[None, :],
+        key_gain[None, :],
+        mixer_gain[None, :],
+        expert_input,
+        expert_ids.T,
+        expert_weights.T,
+        input_gain[None, :],
+        out_gain[None, :],
+    )
+    scratch = [pltpu.VMEM(value.shape, value.dtype) for value in inputs]
+    scratch += [
+        dma((len(inputs),)),
         pltpu.VMEM(w_gate.shape[1:], bf16),
         pltpu.VMEM(w_up.shape[1:], bf16),
         pltpu.VMEM(w_down.shape[1:], bf16),
@@ -1183,9 +1236,9 @@
         (2, 2),
     ):
         scratch += [dma(shape), dma(shape)]
-    return pl.pallas_call(
-        functools.partial(layer_kernel, n_ep, n_x, n_tp, cap),
-        in_specs=[vmem] * 13 + [hbm] * 4,
+    mixer_rows, moe_rows = pl.pallas_call(
+        functools.partial(load_inputs, n_ep, n_x, n_tp, cap, len(inputs)),
+        in_specs=[hbm] * 17,
         out_specs=(vmem, vmem),
         out_shape=(
             jax.ShapeDtypeStruct((own_tokens, width), bf16),
@@ -1193,28 +1246,27 @@
         ),
         scratch_shapes=scratch,
         compiler_params=pltpu.CompilerParams(
-            collective_id=0, has_side_effects=True, vmem_limit_bytes=60 * 1024 * 1024
+            collective_id=0, has_side_effects=True, vmem_limit_bytes=62914560
         ),
         name="layer",
     )(
-        query_rows,
-        key_rows,
-        value_rows,
-        jnp.asarray(row_table),
-        jnp.asarray(col_table),
-        query_gain[None, :],
-        key_gain[None, :],
-        mixer_gain[None, :],
-        expert_input,
-        expert_ids.T,
-        expert_weights.T,
-        input_gain[None, :],
-        out_gain[None, :],
+        *inputs,
         w_gate,
         w_up,
         w_down,
         w_out,
     )
+    return pl.pallas_call(
+        hand_over,
+        in_specs=[vmem] * 2,
+        out_specs=(vmem, vmem),
+        out_shape=(
+            jax.ShapeDtypeStruct(mixer_rows.shape, bf16),
+            jax.ShapeDtypeStruct(moe_rows.shape, bf16),
+        ),
+        compiler_params=pltpu.CompilerParams(vmem_limit_bytes=4 * 1024 * 1024),
+        name="hand_over",
+    )(mixer_rows, moe_rows)
 
 
 def per_device(

time: 87.1 us -> 84.1 us (0.966)
  Pallas kernels: 82.9 us -> 81.3 us
  local copies, waits for them, and re-layouts: 3.38 us -> 1.92 us
    pallas_call x1 -> x2, Pallas kernels: 82.9 us -> 81.3 us  [the longest x1 80.4 us: layer(): pl.pallas_call(functools.partial(load_inputs, n_ep, n_x, n_tp, cap, len(i...]
    unnamed x2 -> x4, local copies, waits for them, and re-layouts: 3.38 us -> 1.92 us
where the time goes in v3:
time: 84.1 us; the launch traced here: 83.9 us
  Pallas kernels  81.3 us (97%)
  local copies, waits for them, and re-layouts  1.92 us (2%)
    pallas_call x1, Pallas kernels, layer(): pl.pallas_call(functools.partial(load_inputs, n_ep, n_x, n_tp, cap, len(i...  80.4 us
    unnamed x4, local copies, waits for them, and re-layouts  1.92 us

profile of v3, /device:TPU:0, one launch (start us, length us, event | category | flops | bytes accessed | tf_op | source)
XLA Modules:
  0.0 83.9 jit_solution(11405626426911040389)
XLA Ops:
  0.6 80.4 %layer.1 = (bf16[96,2048]{1,0:T(8,128)(2,1)}, bf16[192,512]{1,0:T(8,128)(2,1)}) custom-call(bf16[384,1024]{1,0:T(8,128)(2,1)} %refs_0_.1, bf16[384,512]{1,0:T(8,128)(2,1)} %refs_1_.1, bf16[384,512]{1,0:T(8,128)(2,1)} %refs_2_.1, f32[2,48,128]{2,1,0:T(8,128)} %constant.4.clone.refs_3_, f32[2,64,128]{2,1,0:T(8,128)} %constant.5.clone.refs_4_, ...), custom_call_target="tpu_custom_call" | custom-call | tf_op jit(solution)/shard_map/layer/pallas_call | solution.py:1239
  81.1 0.0 copy-start
  81.1 1.0 %copy-done = bf16[96,2048]{1,0:T(8,128)(2,1)S(1)} copy-done((bf16[96,2048]{1,0:T(8,128)(2,1)S(1)}, bf16[96,2048]{1,0:T(8,128)(2,1)}, u32[]{:S(2)}) %copy-start) | copy-done | bytes 393240
  82.1 0.0 copy-start.1
  82.1 0.9 %copy-done.1 = bf16[192,512]{1,0:T(8,128)(2,1)S(1)} copy-done((bf16[192,512]{1,0:T(8,128)(2,1)S(1)}, bf16[192,512]{1,0:T(8,128)(2,1)}, u32[]{:S(2)}) %copy-start.1) | copy-done | bytes 196632
  83.0 0.8 %hand_over.1 = (bf16[96,2048]{1,0:T(8,128)(2,1)}, bf16[192,512]{1,0:T(8,128)(2,1)}) custom-call(bf16[96,2048]{1,0:T(8,128)(2,1)S(1)} %copy-done, bf16[192,512]{1,0:T(8,128)(2,1)S(1)} %copy-done.1), custom_call_target="tpu_custom_call" | custom-call | tf_op jit(solution)/shard_map/hand_over/pallas_call | solution.py:1259
Async XLA Ops:
  81.1 1.0 %copy-start = (bf16[96,2048]{1,0:T(8,128)(2,1)S(1)}, bf16[96,2048]{1,0:T(8,128)(2,1)}, u32[]{:S(2)}) copy-start(bf16[96,2048]{1,0:T(8,128)(2,1)} %get-tuple-element.4.mixer_in) | copy-start | bytes 1179652
  82.1 0.9 %copy-start.1 = (bf16[192,512]{1,0:T(8,128)(2,1)S(1)}, bf16[192,512]{1,0:T(8,128)(2,1)}, u32[]{:S(2)}) copy-start(bf16[192,512]{1,0:T(8,128)(2,1)} %get-tuple-element.5.moe_in) | copy-start | bytes 589828
